TPU v7x, 512 devices: a whole 4x4x16 slice. The times are simulated.
512 devices in a mesh: ep: 32 (over z, core), tp: 16 (over y, x).
Axes of the slice: x: 4, y: 4, z: 16, core: 2. Of those that a mesh axis runs over, the one named last changes fastest.
Arguments:
- residual: bfloat16 [2048, 2048], P('ep', 'tp')
- state_re: float32 [2048, 64, 64], P('ep', 'tp'), may hold values from -4 to 4
- state_im: float32 [2048, 64, 64], P('ep', 'tp'), may hold values from -4 to 4
- mix_gain: float32 [2048], replicated, may hold values from 0.1 to 1.9
- proj_in: bfloat16 [2048, 1024], P(None, 'tp'), may hold values from -0.125 to 0.125
- decay_rate: float32 [64, 64], P('tp'), may hold values from 0.1 to 10
- frequency: float32 [64, 64], P('tp'), may hold values from 0 to 201.06177
- log_step: float32 [64], P('tp'), may hold values from -6.9078 to -2.3026
- input_re: float32 [64, 64, 16], P('tp'), may hold values from -1 to 1
- input_im: float32 [64, 64, 16], P('tp'), may hold values from -1 to 1
- read_re: float32 [64, 16, 64], P('tp'), may hold values from -0.5 to 0.5
- read_im: float32 [64, 16, 64], P('tp'), may hold values from -0.5 to 0.5
- skip_gain: float32 [1024], P('tp'), may hold values from -4 to 4
- glu_weight: bfloat16 [1024, 1024], P(None, 'tp'), may hold values from -0.1875 to 0.1875
- out_proj: bfloat16 [1024, 2048], P(None, 'tp'), may hold values from -0.1875 to 0.1875
- ffn_gain: float32 [2048], replicated, may hold values from 0.1 to 1.9
- router: float32 [2048, 32], replicated, may hold values from -0.125 to 0.125
- gate_weight: bfloat16 [32, 2048, 4096], P('ep', None, 'tp'), may hold values from -0.33007812 to 0.33007812
- up_weight: bfloat16 [32, 2048, 4096], P('ep', None, 'tp'), may hold values from -0.33007812 to 0.33007812
- down_weight: bfloat16 [32, 4096, 2048], P('ep', 'tp'), may hold values from -0.046875 to 0.046875
- route_ids: int32 [2048, 4], P('ep'), may hold values from 0 to 31, all different within a row; in each aligned block of 64 rows (0 to 63, 64 to 127, ...) at most 9 rows name the same one
Outputs:
- layer_out: bfloat16 [2048, 2048], P('ep', 'tp')
- state_re_new: float32 [2048, 64, 64], P('ep', 'tp')
- state_im_new: float32 [2048, 64, 64], P('ep', 'tp')
Inputs may be any that keep to these rules, and one draw needn't show every extreme that they name: `route_ids`: each row names 4 different experts. Within the rows of one ep index (aligned blocks of 64 rows) no expert is named more than 9 times, and in some block some expert is named exactly 9 times.
All inputs are finite; a program needn't handle non-finite values.
Results may differ from a plain program's by a relative error of at most 0.014.
Values may be sent and summed in bfloat16 or wider, within the bound.
No kernel may reach another device: no remote copies, remote signals or barrier semaphores. Data moves between devices by JAX's collectives and lax.ppermute only.
A program may use at most 64 MiB of HBM per device.

v0:
```python
import functools

import jax
import jax.numpy as jnp
from jax import lax
from jax.sharding import Mesh
from jax.sharding import PartitionSpec as P

TP = ("tp_0", "tp_1")


EPSILON = 1e-05
LIMIT = 7.0
ALPHA = 1.702


def laid_out(blocks, dim):
    lengths = list(blocks.shape[1:])
    lengths[dim] *= blocks.shape[0]
    return jnp.moveaxis(blocks, 0, dim).reshape(lengths)


def sent_to_all(shard, axis):
    length = lax.axis_size(axis)
    return lax.all_to_all(
        jnp.broadcast_to(shard[None], (length, *shard.shape)), axis, 0, 0, tiled=True
    )


def gather_directly(shard, axis, dim):
    return laid_out(sent_to_all(shard, axis), dim)


def one_axis_at_a_time(shard, axes):
    return functools.reduce(lax.psum, axes, shard)


def split_up(shard, dim, length):
    before, after = (shard.shape[:dim], shard.shape[dim + 1 :])
    return jnp.moveaxis(shard.reshape(*before, length, -1, *after), dim, 0)


def sum_at_owner(shard, axis, dim):
    blocks = split_up(shard, dim, lax.axis_size(axis))
    arrived = lax.all_to_all(blocks, axis, split_axis=0, concat_axis=0, tiled=True)
    return arrived.astype(jnp.float32).sum(axis=0)


def discretise(decay_rate, frequency, log_step, input_re, input_im):
    real_part = -decay_rate
    step_size = jnp.exp(log_step)[:, None]
    magnitude = jnp.exp(step_size * real_part)
    abar_re = magnitude * jnp.cos(step_size * frequency)
    abar_im = magnitude * jnp.sin(step_size * frequency)
    denom = real_part * real_part + frequency * frequency
    minus_one = abar_re - 1.0
    coef_re = (minus_one * real_part + abar_im * frequency) / denom
    coef_im = (abar_im * real_part - minus_one * frequency) / denom
    bbar_re = coef_re[..., None] * input_re - coef_im[..., None] * input_im
    bbar_im = coef_re[..., None] * input_im + coef_im[..., None] * input_re
    return (abar_re, abar_im, bbar_re, bbar_im)


def per_device(
    residual,
    state_re,
    state_im,
    mix_gain,
    proj_in,
    decay_rate,
    frequency,
    log_step,
    input_re,
    input_im,
    read_re,
    read_im,
    skip_gain,
    glu_weight,
    out_proj,
    ffn_gain,
    router,
    gate_weight,
    up_weight,
    down_weight,
    route_ids,
):
    high = lax.Precision.HIGHEST
    seq_rows = residual.shape[0]
    col_count = residual.shape[1]
    width = mix_gain.shape[0]
    ep_size = lax.axis_size("ep")
    col_start = lax.axis_index(TP) * col_count
    own_resid = residual.astype(jnp.float32)
    full_resid = gather_directly(residual, TP, 1).astype(jnp.float32)
    scale_one = lax.rsqrt(jnp.mean(full_resid * full_resid, axis=1, keepdims=True) + EPSILON)
    xnorm = (full_resid * scale_one * mix_gain).astype(jnp.bfloat16)
    mix_in = jnp.dot(xnorm, proj_in, preferred_element_type=jnp.float32).astype(jnp.bfloat16)
    mix_f = mix_in.astype(jnp.float32)
    group_count = decay_rate.shape[0]
    group_width = input_re.shape[2]
    grouped = mix_f.reshape(seq_rows, group_count, group_width)
    abar_re, abar_im, bbar_re, bbar_im = discretise(
        decay_rate, frequency, log_step, input_re, input_im
    )
    drive_re = jnp.einsum("sgc,gnc->sgn", grouped, bbar_re, precision=high)
    drive_im = jnp.einsum("sgc,gnc->sgn", grouped, bbar_im, precision=high)
    state_re_new = abar_re * state_re - abar_im * state_im + drive_re
    state_im_new = abar_re * state_im + abar_im * state_re + drive_im
    readout = jnp.einsum("sgn,gcn->sgc", state_re_new, read_re, precision=high) - jnp.einsum(
        "sgn,gcn->sgc", state_im_new, read_im, precision=high
    )
    mixer = jax.nn.gelu(
        readout.reshape(seq_rows, group_count * group_width) + skip_gain * mix_f, approximate=False
    )
    all_mixer = gather_directly(mixer.astype(jnp.bfloat16), TP, 1)
    glu_gate = jnp.dot(all_mixer, glu_weight, preferred_element_type=jnp.float32)
    gated = (mixer * jax.nn.sigmoid(glu_gate)).astype(jnp.bfloat16)
    all_gated = gather_directly(gated, TP, 1)
    mixed = jnp.dot(all_gated, out_proj, preferred_element_type=jnp.float32)
    stream = (own_resid + mixed).astype(jnp.bfloat16)
    stream_f = stream.astype(jnp.float32)
    gain_own = lax.dynamic_slice_in_dim(ffn_gain, col_start, col_count, 0)
    router_own = lax.dynamic_slice_in_dim(router, col_start, col_count, 0)
    squares, partial_logits = (
        one_axis_at_a_time(jnp.sum(stream_f * stream_f, axis=1), TP),
        one_axis_at_a_time(jnp.dot(stream_f * gain_own, router_own, precision=high), TP),
    )
    inverse = lax.rsqrt(squares / width + EPSILON)[:, None]
    logits = partial_logits * inverse
    payload = (stream_f * inverse * gain_own).astype(jnp.bfloat16)
    expert_count = router.shape[1]
    top_count = route_ids.shape[1]
    capacity = seq_rows * top_count // expert_count + 1
    expert_iota = jnp.arange(expert_count, dtype=jnp.int32)
    choose = (route_ids[:, :, None] == expert_iota).astype(jnp.float32)
    picked = jnp.sum(choose * logits[:, None, :], axis=2)
    expon = jnp.exp(picked)
    weights = expon / jnp.sum(expon, axis=1, keepdims=True)
    flat_route = route_ids.reshape(seq_rows * top_count)
    one_hot = (flat_route[:, None] == expert_iota).astype(jnp.int32)
    before = jnp.cumsum(one_hot, axis=0) - one_hot
    slot_ids = jnp.sum(before * one_hot, axis=1)
    target = flat_route * capacity + slot_ids
    slot_iota = jnp.arange(expert_count * capacity, dtype=jnp.int32)
    placing = jnp.any(slot_iota[:, None, None] == target.reshape(seq_rows, top_count)[None], axis=2)
    buffer = jnp.dot(placing.astype(jnp.bfloat16), payload, preferred_element_type=jnp.float32)
    buffer = buffer.astype(jnp.bfloat16).reshape(expert_count, capacity, payload.shape[1])
    local_experts = gate_weight.shape[0]
    full_tokens = gather_directly(
        lax.all_to_all(buffer, "ep", split_axis=0, concat_axis=0, tiled=True), TP, 2
    )
    items = full_tokens.shape[1]
    tokens = full_tokens.reshape(ep_size, local_experts, items, width)
    tokens = tokens.transpose(1, 0, 2, 3).reshape(local_experts, ep_size * items, width)
    gate_pre = jnp.einsum("esd,edf->esf", tokens, gate_weight, preferred_element_type=jnp.float32)
    up_pre = jnp.einsum("esd,edf->esf", tokens, up_weight, preferred_element_type=jnp.float32)
    gate_cl = jnp.minimum(gate_pre, LIMIT)
    up_cl = jnp.clip(up_pre, -LIMIT, LIMIT)
    active = ((up_cl + 1.0) * (gate_cl * jax.nn.sigmoid(ALPHA * gate_cl))).astype(jnp.bfloat16)
    partial_value = jnp.einsum(
        "esf,efd->esd", active, down_weight, preferred_element_type=jnp.float32
    ).astype(jnp.bfloat16)
    summed = sum_at_owner(partial_value.astype(jnp.float32).astype(jnp.bfloat16), TP, 2).astype(
        jnp.bfloat16
    )
    outgoing = summed.reshape(local_experts, ep_size, items, col_count)
    outgoing = outgoing.transpose(1, 0, 2, 3).reshape(ep_size * local_experts, items, col_count)
    returned = lax.all_to_all(outgoing, "ep", split_axis=0, concat_axis=0, tiled=True)
    flat_back = returned.reshape(expert_count * capacity, col_count)
    fetched = (
        jnp.take(flat_back, target, axis=0)
        .astype(jnp.float32)
        .reshape(seq_rows, top_count, col_count)
    )
    experts_sum = jnp.sum(weights[..., None] * fetched, axis=1)
    layer_out = (stream_f + experts_sum).astype(jnp.bfloat16)
    return (layer_out, state_re_new, state_im_new)


def solution(mesh):
    split = Mesh(mesh.devices.reshape(mesh.shape["ep"], 4, 4), ("ep", "tp_0", "tp_1"))
    in_specs = (
        P("ep", TP),
        P("ep", TP, None),
        P("ep", TP, None),
        P(),
        P(None, TP),
        P(TP, None),
        P(TP, None),
        P(TP),
        P(TP, None, None),
        P(TP, None, None),
        P(TP, None, None),
        P(TP, None, None),
        P(TP),
        P(None, TP),
        P(None, TP),
        P(),
        P(),
        P("ep", None, TP),
        P("ep", None, TP),
        P("ep", TP, None),
        P("ep", None),
    )
    out_specs = (P("ep", TP), P("ep", TP, None), P("ep", TP, None))
    return jax.shard_map(
        per_device, mesh=split, in_specs=in_specs, out_specs=out_specs, check_vma=False
    )
```

profile of v0, /device:TPU:1, one launch (start us, length us, event | category | flops | bytes accessed | tf_op | source)
XLA Modules:
  0.0 187.0 jit_solution(13639931999646253795)
XLA Ops:
  0.7 1.6 broadcast_in_dim.15
  2.3 7.7 %all-to-all-start = ((bf16[16,64,128]{2,1,0:T(8,128)(2,1)}), bf16[16,64,128]{2,1,0:T(8,128)(2,1)S(1)}, u32[]{:S(2)}, u32[]{:S(2)}) async-start(bf16[16,64,128]{2,1,0:T(8,128)(2,1)} %broadcast_in_dim.15), calls=%async_computation | async-start | bytes 524288 | tf_op jit(solution)/shard_map/all_to_all | solution.py:25
  10.0 0.8 copy.132
  10.9 1.0 copy.121
  12.0 0.6 reduce-window.6
  12.8 4.9 %all-to-all-done = bf16[16,64,128]{2,1,0:T(8,128)(2,1)S(1)} async-done(((bf16[16,64,128]{2,1,0:T(8,128)(2,1)}), bf16[16,64,128]{2,1,0:T(8,128)(2,1)S(1)}, u32[]{:S(2)}, u32[]{:S(2)}) %all-to-all-start) | async-done | bytes 262176 | tf_op jit(solution)/shard_map/all_to_all | solution.py:25
  17.9 0.3 convolution_convert_fusion.2
  18.3 0.3 fusion.20
  18.6 0.3 fusion.21
  18.9 0.2 fusion.93
  19.1 0.2 convolution_subtract_fusion
  19.6 0.9 reshape.198
  20.5 3.5 %all-to-all-start.1 = ((bf16[16,2,2048]{2,1,0:T(2,128)(2,1)}), bf16[16,2,2048]{2,1,0:T(2,128)(2,1)S(1)}, u32[]{:S(2)}, u32[]{:S(2)}) async-start(bf16[16,2,2048]{2,1,0:T(2,128)(2,1)} %reshape.198), calls=%async_computation.1 | async-start | bytes 262144 | tf_op jit(solution)/shard_map/all_to_all | solution.py:25
  24.1 0.2 slice_reduce_fusion
  24.7 6.2 %all-to-all-done.1 = bf16[16,2,2048]{2,1,0:T(2,128)(2,1)S(1)} async-done(((bf16[16,2,2048]{2,1,0:T(2,128)(2,1)}), bf16[16,2,2048]{2,1,0:T(2,128)(2,1)S(1)}, u32[]{:S(2)}, u32[]{:S(2)}) %all-to-all-start.1) | async-done | bytes 131104 | tf_op jit(solution)/shard_map/all_to_all | solution.py:25
  30.9 0.2 reshape.199
  31.1 0.2 copy.129
  31.3 0.2 reshape.177
  31.5 0.2 fusion.26
  31.8 0.9 reshape.200
  32.7 3.5 %all-to-all-start.2 = ((bf16[16,2,2048]{2,1,0:T(2,128)(2,1)}), bf16[16,2,2048]{2,1,0:T(2,128)(2,1)S(1)}, u32[]{:S(2)}, u32[]{:S(2)}) async-start(bf16[16,2,2048]{2,1,0:T(2,128)(2,1)} %reshape.200), calls=%async_computation.2 | async-start | bytes 262144 | tf_op jit(solution)/shard_map/all_to_all | solution.py:25
  36.2 0.8 dynamic_slice.6
  37.1 5.9 %all-to-all-done.2 = bf16[16,2,2048]{2,1,0:T(2,128)(2,1)S(1)} async-done(((bf16[16,2,2048]{2,1,0:T(2,128)(2,1)}), bf16[16,2,2048]{2,1,0:T(2,128)(2,1)S(1)}, u32[]{:S(2)}, u32[]{:S(2)}) %all-to-all-start.2) | async-done | bytes 131104 | tf_op jit(solution)/shard_map/all_to_all | solution.py:25
  43.0 0.2 reshape.201
  43.4 0.2 reshape.178
  43.6 0.3 multiply_reduce_fusion.1
  43.9 0.9 fusion.60
  44.8 11.3 %all-reduce.1 = (f32[64]{0:T(128)S(1)}, f32[64,32]{0,1:T(8,128)S(1)}) all-reduce(f32[64]{0:T(128)S(1)} %get-tuple-element.33, f32[64,32]{0,1:T(8,128)S(1)} %fusion.60), channel_id=1, replica_groups=mesh['ep'=32,'tp_0'=4,'tp_1'=4] {'tp_0'}, use_global_device_ids=true, to_apply=%region_4.0 | all-reduce | flops 2112 | bytes 16896 | tf_op jit(solution)/shard_map/psum | solution.py:35
  56.1 12.7 %all-reduce = (f32[64]{0:T(128)S(1)}, f32[64,32]{0,1:T(8,128)}) all-reduce(f32[64]{0:T(128)S(1)} %get-tuple-element.23, f32[64,32]{0,1:T(8,128)S(1)} %get-tuple-element.24), channel_id=1, replica_groups=mesh['ep'=32,'tp_0'=4,'tp_1'=4] {'tp_1'}, use_global_device_ids=true, to_apply=%region_5.0 | all-reduce | flops 2112 | bytes 16896 | tf_op jit(solution)/shard_map/psum | solution.py:35
  68.9 0.3 convolution_convert_fusion.1
  69.2 42.2 %all_to_all.35 = bf16[32,9,128]{2,1,0:T(8,128)(2,1)S(1)} all-to-all(bf16[32,9,128]{2,1,0:T(8,128)(2,1)S(1)} %reshape.181), channel_id=1, replica_groups=mesh['ep'=32,'tp_0'=4,'tp_1'=4] {'ep'}, dimensions={0} | all-to-all | bytes 147456 | tf_op jit(solution)/shard_map/all_to_all | solution.py:150
  111.5 20.2 %all_to_all.36 = bf16[16,32,9,128]{3,1,2,0:T(8,128)(2,1)S(1)} all-to-all(bf16[16,32,9,128]{3,1,2,0:T(8,128)(2,1)S(1)} %broadcast_in_dim.19), channel_id=1, replica_groups=mesh['ep'=32,'tp_0'=4,'tp_1'=4] {'tp_0','tp_1'}, dimensions={0} | all-to-all | bytes 2359296 | tf_op jit(solution)/shard_map/all_to_all | solution.py:25
  131.7 0.5 copy.138
  132.2 0.8 copy-done.17
  132.9 1.2 fusion.11
  134.1 2.7 %fusion = bf16[36,8,16,128]{3,1,2,0:T(8,128)(2,1)S(1)} fusion(bf16[1,256,2048]{2,1,0:T(8,128)(2,1)S(1)} %copy-done, bf16[1,2048,256]{2,1,0:T(8,128)(2,1)} %param.39, bf16[36,8,16,128]{3,2,1,0:T(8,128)(2,1)S(1)} %bitcast.101, f32[288,256]{1,0:T(8,128)} %fusion.11), kind=kOutput, calls=%fused_computation.2 | convolution fusion | flops 605233152 | bytes 4751360 | tf_op jit(solution)/shard_map/esf,efd->esd/dot_general | solution.py:160
  136.8 0.2 copy.148
  137.1 1.3 copy.163
  138.4 3.8 %all-to-all-start.5 = ((bf16[16,1,288,128]{3,2,1,0:T(8,128)(2,1)}), bf16[16,1,288,128]{3,2,1,0:T(8,128)(2,1)S(1)}, u32[]{:S(2)}, u32[]{:S(2)}) async-start(bf16[16,1,288,128]{3,2,1,0:T(8,128)(2,1)} %bitcast.97), calls=%async_computation.5 | async-start | bytes 2359296 | tf_op jit(solution)/shard_map/all_to_all | solution.py:45
  142.6 0.8 copy.141
  143.4 0.8 copy.142
  144.2 14.2 %all-to-all-done.5 = bf16[16,1,288,128]{3,2,1,0:T(8,128)(2,1)S(1)} async-done(((bf16[16,1,288,128]{3,2,1,0:T(8,128)(2,1)}), bf16[16,1,288,128]{3,2,1,0:T(8,128)(2,1)S(1)}, u32[]{:S(2)}, u32[]{:S(2)}) %all-to-all-start.5) | async-done | bytes 1179680 | tf_op jit(solution)/shard_map/all_to_all | solution.py:45
  158.5 0.7 reshape_transpose_reshape.3
  159.2 10.2 %all-to-all-start.6 = ((bf16[32,9,128]{2,1,0:T(8,128)(2,1)}), bf16[32,9,128]{2,1,0:T(8,128)(2,1)S(1)}, u32[]{:S(2)}, u32[]{:S(2)}) async-start(bf16[32,9,128]{2,1,0:T(8,128)(2,1)} %reshape_transpose_reshape.3), calls=%async_computation.6 | async-start | bytes 262144 | tf_op jit(solution)/shard_map/all_to_all | solution.py:168
  169.5 15.7 %all-to-all-done.6 = bf16[32,9,128]{2,1,0:T(8,128)(2,1)S(1)} async-done(((bf16[32,9,128]{2,1,0:T(8,128)(2,1)}), bf16[32,9,128]{2,1,0:T(8,128)(2,1)S(1)}, u32[]{:S(2)}, u32[]{:S(2)}) %all-to-all-start.6) | async-done | bytes 73760 | tf_op jit(solution)/shard_map/all_to_all | solution.py:168
  185.3 0.9 gather_fusion
  186.2 0.2 multiply_reduce_fusion
  186.4 0.6 add_convert_fusion
  (81 shorter events, 2.6 us)
Async XLA Ops:
  0.6 133.5 %copy-start = (bf16[1,256,2048]{2,1,0:T(8,128)(2,1)S(1)}, bf16[1,256,2048]{2,1,0:T(8,128)(2,1)}, u32[]{:S(2)}) copy-start(bf16[1,256,2048]{2,1,0:T(8,128)(2,1)} %param.40) | copy-start | bytes 3145732
  0.6 11.2 %copy-start.6 = (f32[64,4,64]{2,1,0:T(4,128)S(1)}, f32[64,4,64]{2,1,0:T(4,128)}, u32[]{:S(2)}) copy-start(f32[64,4,64]{2,1,0:T(4,128)} %param.22) | copy-start | bytes 196612
  0.7 11.4 %copy-start.21 = (f32[4]{0:T(128)S(1)}, f32[4]{0:T(128)}, u32[]{:S(2)}) copy-start(f32[4]{0:T(128)} %param.28) | copy-start | bytes 52
  0.7 12.0 %copy-start.14 = (f32[4,64]{1,0:T(4,128)S(1)}, f32[4,64]{1,0:T(4,128)}, u32[]{:S(2)}) copy-start(f32[4,64]{1,0:T(4,128)} %param.27) | copy-start | bytes 3076
  0.7 12.0 %copy-start.15 = (f32[4,64]{1,0:T(4,128)S(1)}, f32[4,64]{1,0:T(4,128)}, u32[]{:S(2)}) copy-start(f32[4,64]{1,0:T(4,128)} %param.26) | copy-start | bytes 3076
  0.7 17.2 %copy-start.18 = (bf16[2048,64]{0,1:T(8,128)(2,1)S(1)}, bf16[2048,64]{0,1:T(8,128)(2,1)}, u32[]{:S(2)}) copy-start(bf16[2048,64]{0,1:T(8,128)(2,1)} %param.25) | copy-start | bytes 786436
  0.7 17.2 %copy-start.20 = (f32[2048]{0:T(1024)S(1)}, f32[2048]{0:T(1024)}, u32[]{:S(2)}) copy-start(f32[2048]{0:T(1024)} %param.24) | copy-start | bytes 24580
  2.3 16.0 %copy-start.7 = (f32[4,64,16]{1,2,0:T(8,128)S(1)}, f32[4,64,16]{1,2,0:T(8,128)}, u32[]{:S(2)}) copy-start(f32[4,64,16]{1,2,0:T(8,128)} %param.30) | copy-start | bytes 49156
  2.3 16.0 %copy-start.8 = (f32[4,64,16]{1,2,0:T(8,128)S(1)}, f32[4,64,16]{1,2,0:T(8,128)}, u32[]{:S(2)}) copy-start(f32[4,64,16]{1,2,0:T(8,128)} %param.29) | copy-start | bytes 49156
  2.3 15.4 %all-to-all-start = ((bf16[16,64,128]{2,1,0:T(8,128)(2,1)}), bf16[16,64,128]{2,1,0:T(8,128)(2,1)S(1)}, u32[]{:S(2)}, u32[]{:S(2)}) async-start(bf16[16,64,128]{2,1,0:T(8,128)(2,1)} %broadcast_in_dim.15), calls=%async_computation | async-start | bytes 524288 | tf_op jit(solution)/shard_map/all_to_all | solution.py:25
  11.9 7.0 %copy-start.12 = (f32[4,16,64]{2,1,0:T(8,128)S(1)}, f32[4,16,64]{2,1,0:T(8,128)}, u32[]{:S(2)}) copy-start(f32[4,16,64]{2,1,0:T(8,128)} %param.31) | copy-start | bytes 49156
  12.0 7.1 %copy-start.10 = (f32[4,16,64]{2,1,0:T(8,128)S(1)}, f32[4,16,64]{2,1,0:T(8,128)}, u32[]{:S(2)}) copy-start(f32[4,16,64]{2,1,0:T(8,128)} %param.32) | copy-start | bytes 49156
  17.8 1.6 copy-start.16
  18.6 12.5 %copy-start.1 = (f32[64,4,64]{0,2,1:T(8,128)}, f32[64,4,64]{0,2,1:T(8,128)S(1)}, u32[]{:S(2)}) copy-start(f32[64,4,64]{0,2,1:T(8,128)S(1)} %fusion.20) | copy-start | bytes 196612
  19.6 11.9 %copy-start.19 = (bf16[1024,64]{0,1:T(8,128)(2,1)S(1)}, bf16[1024,64]{0,1:T(8,128)(2,1)}, u32[]{:S(2)}) copy-start(bf16[1024,64]{0,1:T(8,128)(2,1)} %param.34) | copy-start | bytes 393220
  20.5 10.3 %all-to-all-start.1 = ((bf16[16,2,2048]{2,1,0:T(2,128)(2,1)}), bf16[16,2,2048]{2,1,0:T(2,128)(2,1)S(1)}, u32[]{:S(2)}, u32[]{:S(2)}) async-start(bf16[16,2,2048]{2,1,0:T(2,128)(2,1)} %reshape.198), calls=%async_computation.1 | async-start | bytes 262144 | tf_op jit(solution)/shard_map/all_to_all | solution.py:25
  31.1 5.1 %copy-start.11 = (s32[64,4]{0,1:T(4,128)S(1)}, s32[64,4]{0,1:T(4,128)}, u32[]{:S(2)}) copy-start(s32[64,4]{0,1:T(4,128)} %param.41) | copy-start | bytes 3076
  31.7 11.9 %copy-start.5 = (bf16[1024,128]{1,0:T(8,128)(2,1)S(1)}, bf16[1024,128]{1,0:T(8,128)(2,1)}, u32[]{:S(2)}) copy-start(bf16[1024,128]{1,0:T(8,128)(2,1)} %param.35) | copy-start | bytes 786436
  31.7 11.9 %copy-start.9 = (bf16[64,128]{1,0:T(8,128)(2,1)S(1)}, bf16[64,128]{1,0:T(8,128)(2,1)}, u32[]{:S(2)}) copy-start(bf16[64,128]{1,0:T(8,128)(2,1)} %param.21) | copy-start | bytes 49156
  32.7 10.3 %all-to-all-start.2 = ((bf16[16,2,2048]{2,1,0:T(2,128)(2,1)}), bf16[16,2,2048]{2,1,0:T(2,128)(2,1)S(1)}, u32[]{:S(2)}, u32[]{:S(2)}) async-start(bf16[16,2,2048]{2,1,0:T(2,128)(2,1)} %reshape.200), calls=%async_computation.2 | async-start | bytes 262144 | tf_op jit(solution)/shard_map/all_to_all | solution.py:25
  43.9 25.2 %copy-start.3 = (f32[64,128]{1,0:T(8,128)}, f32[64,128]{1,0:T(8,128)S(1)}, u32[]{:S(2)}) copy-start(f32[64,128]{1,0:T(8,128)S(1)} %get-tuple-element.34) | copy-start | bytes 98308
  131.7 1.2 copy-start.17
  138.4 4.2 %copy-start.2 = (f32[64,4,64]{0,2,1:T(8,128)S(1)}, f32[64,4,64]{0,2,1:T(8,128)}, u32[]{:S(2)}) copy-start(f32[64,4,64]{0,2,1:T(8,128)} %copy-done.1) | copy-start | bytes 196612
  138.4 5.7 %copy-start.13 = (f32[64,32]{0,1:T(8,128)S(1)}, f32[64,32]{0,1:T(8,128)}, u32[]{:S(2)}) copy-start(f32[64,32]{0,1:T(8,128)} %get-tuple-element.22) | copy-start | bytes 24580
  138.4 19.9 %all-to-all-start.5 = ((bf16[16,1,288,128]{3,2,1,0:T(8,128)(2,1)}), bf16[16,1,288,128]{3,2,1,0:T(8,128)(2,1)S(1)}, u32[]{:S(2)}, u32[]{:S(2)}) async-start(bf16[16,1,288,128]{3,2,1,0:T(8,128)(2,1)} %bitcast.97), calls=%async_computation.5 | async-start | bytes 2359296 | tf_op jit(solution)/shard_map/all_to_all | solution.py:45
  144.2 42.2 %copy-start.4 = (f32[64,128]{1,0:T(8,128)S(1)}, f32[64,128]{1,0:T(8,128)}, u32[]{:S(2)}) copy-start(f32[64,128]{1,0:T(8,128)} %copy-done.3) | copy-start | bytes 98308
  159.2 26.1 %all-to-all-start.6 = ((bf16[32,9,128]{2,1,0:T(8,128)(2,1)}), bf16[32,9,128]{2,1,0:T(8,128)(2,1)S(1)}, u32[]{:S(2)}, u32[]{:S(2)}) async-start(bf16[32,9,128]{2,1,0:T(8,128)(2,1)} %reshape_transpose_reshape.3), calls=%async_computation.6 | async-start | bytes 262144 | tf_op jit(solution)/shard_map/all_to_all | solution.py:168
where the time goes:
time: 188 us; the launch traced here: 187 us
  blocking collectives  86.4 us (46%)
  waiting for transfers between devices  46.9 us (25%)
  starting transfers between devices  28.8 us (15%)
  local copies, waits for them, and re-layouts  14.6 us (8%)
  matrix products  6.81 us (4%)
  other arithmetic  2.29 us (1%)
    all_to_all x1, blocking collectives, per_device(): lax.all_to_all(buffer, 'ep', split_axis=0, concat_axis=0, tiled=True)  42.2 us
    psum x2, blocking collectives, one_axis_at_a_time(): return functools.reduce(lax.psum, axes, shard)  24.1 us
    all_to_all x1, blocking collectives, sent_to_all(): lax.all_to_all(jnp.broadcast_to(shard[None], (length, *shard.shape)), axi...  20.2 us
    all_to_all x3, waiting for transfers between devices, sent_to_all(): lax.all_to_all(jnp.broadcast_to(shard[None], (length, *shard.shape)), axi...  17 us
    all_to_all x1, waiting for transfers between devices, per_device(): lax.all_to_all(outgoing, 'ep', split_axis=0, concat_axis=0, tiled=True)  15.7 us
    all_to_all x3, starting transfers between devices, sent_to_all(): lax.all_to_all(jnp.broadcast_to(shard[None], (length, *shard.shape)), axi...  14.7 us
    all_to_all x1, waiting for transfers between devices, sum_at_owner(): lax.all_to_all(blocks, axis, split_axis=0, concat_axis=0, tiled=True)  14.2 us
    all_to_all x1, starting transfers between devices, per_device(): lax.all_to_all(outgoing, 'ep', split_axis=0, concat_axis=0, tiled=True)  10.2 us
  transfers between devices with their start and end apart: 5, of which 5 were waited for; matrix products, arithmetic and copies ran while one was open for 3% of the time, Pallas kernels for 0%

commit v1 on v0

v1 whole, which is shorter than its diff:
```python
import functools

import jax
import jax.numpy as jnp
from jax import lax
from jax.experimental import pallas as pl
from jax.experimental.pallas import tpu as pltpu
from jax.sharding import Mesh
from jax.sharding import PartitionSpec as P

TP = ("tp_0", "tp_1")
EPSILON = 1e-05
LIMIT = 7.0
ALPHA = 1.702
F32 = jnp.float32
BF16 = jnp.bfloat16
TILE = 128


def call(body, out, *args, mib=16, **settings):
    return pl.pallas_call(
        body,
        out_shape=out,
        compiler_params=pltpu.CompilerParams(vmem_limit_bytes=mib << 20),
        **settings,
    )(*args)


def shape_of(shape, dtype):
    return jax.ShapeDtypeStruct(shape, dtype)


def halves(value):
    high = value.astype(BF16)
    return high, (value - high.astype(F32)).astype(BF16)


def dot(left, right):
    return jnp.dot(left, right, preferred_element_type=F32)


def dot_rows(left, right):
    return lax.dot_general(left, right, (((1,), (1,)), ((), ())), preferred_element_type=F32)


def exchange(blocks, axis):
    return lax.all_to_all(blocks, axis, 0, 0, tiled=True)


def discretise(decay_rate, frequency, log_step, input_re, input_im):
    real_part = -decay_rate
    step_size = jnp.exp(log_step)[:, None]
    magnitude = jnp.exp(step_size * real_part)
    abar_re = magnitude * jnp.cos(step_size * frequency)
    abar_im = magnitude * jnp.sin(step_size * frequency)
    denom = real_part * real_part + frequency * frequency
    minus_one = abar_re - 1.0
    coef_re = (minus_one * real_part + abar_im * frequency) / denom
    coef_im = (abar_im * real_part - minus_one * frequency) / denom
    bbar_re = coef_re[:, None] * input_re - coef_im[:, None] * input_im
    bbar_im = coef_re[:, None] * input_im + coef_im[:, None] * input_re
    return (abar_re, abar_im, bbar_re, bbar_im)


def block_diagonal(blocks):
    count, rows, cols = blocks.shape
    flat = blocks.reshape(count * rows, cols)
    wide = jnp.concatenate([flat] * count, axis=1)
    row_block = lax.broadcasted_iota(jnp.int32, wide.shape, 0) // rows
    col_block = lax.broadcasted_iota(jnp.int32, wide.shape, 1) // cols
    return jnp.where(row_block == col_block, wide, 0.0)


def packed(value):
    half = value.shape[0] // 2
    return jnp.concatenate([value[:half], value[half:]], axis=1)


def unpacked(ref):
    peers, half, lanes = ref.shape
    width = lanes // 2
    left = lax.broadcasted_iota(jnp.int32, (half, lanes), 1) < width
    top, bottom = [], []
    for pair in range(peers // 2):
        one = ref[2 * pair].astype(F32)
        two = ref[2 * pair + 1].astype(F32)
        top.append(jnp.where(left, one, pltpu.roll(two, width, 1)))
        bottom.append(jnp.where(left, pltpu.roll(one, width, 1), two))
    rows = [jnp.concatenate(top, axis=1), jnp.concatenate(bottom, axis=1)]
    return jnp.concatenate(rows, axis=0).astype(BF16)


def routing_kernel(per, cap, experts, route_ref, across_ref, place_ref, fetch_ref, pick_ref, keep_ref, grow_ref, tag_ref):
    seqs, top = route_ref.shape
    slots = place_ref.shape[0]
    rows = keep_ref.shape[0]
    route = route_ref[...]
    across = across_ref[...]

    def iota(shape, dim):
        return lax.broadcasted_iota(jnp.int32, shape, dim)

    expert_lane = iota((seqs, experts), 1)
    expert_row = iota((experts, seqs), 0)
    named = sum((route[:, k : k + 1] == expert_lane).astype(F32) for k in range(top))
    named_across = sum((across[k : k + 1, :] == expert_row).astype(F32) for k in range(top))
    earlier = (iota((seqs, seqs), 1) < iota((seqs, seqs), 0)).astype(BF16)
    earlier_across = (iota((seqs, seqs), 0) < iota((seqs, seqs), 1)).astype(BF16)
    count = dot(earlier, named.astype(BF16))
    count_across = dot(named_across.astype(BF16), earlier_across)
    slot_row = iota((slots, seqs), 0)
    slot_lane = iota((seqs, slots), 1)
    lane = iota((seqs, TILE), 1)
    place = jnp.zeros((slots, seqs), F32)
    for k in range(top):
        chosen = route[:, k : k + 1]
        slot = jnp.sum(jnp.where(chosen == expert_lane, count, 0.0), axis=1, keepdims=True).astype(jnp.int32)
        fetch_ref[k * seqs : (k + 1) * seqs, :] = (slot_lane == chosen * per + slot).astype(F32).astype(BF16)
        fetch_ref[(top + k) * seqs : (top + k + 1) * seqs, :] = (
            (slot_lane == chosen * per + cap).astype(F32).astype(BF16)
        )
        pick_ref[k * seqs : (k + 1) * seqs, :] = ((lane == slot) | (lane == slot + 16)).astype(F32)
        chosen_across = across[k : k + 1, :]
        slot_across = jnp.sum(
            jnp.where(chosen_across == expert_row, count_across, 0.0), axis=0, keepdims=True
        ).astype(jnp.int32)
        place = place + (slot_row == chosen_across * per + slot_across).astype(F32)
    place_ref[...] = place.astype(BF16)
    row = iota((rows, slots), 0)
    keep_ref[...] = (iota((rows, slots), 1) == row + ninth(row)).astype(F32).astype(BF16)
    col = iota((slots, rows), 1)
    grow_ref[...] = (iota((slots, rows), 0) == col + ninth(col)).astype(F32).astype(BF16)
    tag_ref[...] = (iota((slots, rows), 0) == ninth(col) * per + cap).astype(F32).astype(BF16)


def ninth(value):
    return (value * 7282) >> 16


def mixer_kernel(
    resid_ref, gain_ref, proj_ref, state_re_ref, state_im_ref, abar_re_ref, abar_im_ref,
    input_re_ref, input_im_ref, read_re_ref, read_im_ref, skip_ref,
    new_re_ref, new_im_ref, mixer_ref, send_ref,
):
    peers, seqs, cols = resid_ref.shape
    square = jnp.zeros((seqs, cols), F32)
    for t in range(peers):
        part = resid_ref[t].astype(F32)
        square = square + part * part
    mean = jnp.sum(square, axis=1, keepdims=True) / (peers * cols)
    scale = lax.rsqrt(mean + EPSILON)
    normed = jnp.concatenate(
        [(resid_ref[t].astype(F32) * scale * gain_ref[t : t + 1, :]).astype(BF16) for t in range(peers)], axis=1
    )
    mix = dot_rows(normed, proj_ref[...]).astype(BF16)
    width = state_re_ref.shape[1]

    def driven(ref):
        high, low = halves(ref[...])
        return dot(mix, high) + dot(mix, low)

    old_re, old_im = state_re_ref[...], state_im_ref[...]
    abar_re, abar_im = abar_re_ref[...], abar_im_ref[...]
    new_re = abar_re * old_re - abar_im * old_im + driven(input_re_ref)
    new_im = abar_re * old_im + abar_im * old_re + driven(input_im_ref)
    new_re_ref[...] = new_re
    new_im_ref[...] = new_im

    def read(value, ref):
        high, low = halves(value)
        read_high, read_low = halves(ref[...])
        return dot_rows(high, read_high) + dot_rows(high, read_low) + dot_rows(low, read_high)

    value = read(new_re, read_re_ref) - read(new_im, read_im_ref) + skip_ref[...] * mix.astype(F32)
    mixer = 0.5 * value * (1.0 + lax.erf(value * 0.7071067811865476))
    mixer_ref[...] = mixer
    sent = packed(mixer).astype(BF16)
    for t in range(peers):
        send_ref[t] = sent


def gate_kernel(all_ref, weight_ref, mixer_ref, send_ref):
    gate = dot_rows(unpacked(all_ref), weight_ref[...])
    gated = packed(mixer_ref[...] * jax.nn.sigmoid(gate)).astype(BF16)
    for t in range(send_ref.shape[0]):
        send_ref[t] = gated


def stream_kernel(all_ref, weight_ref, resid_ref, place_ref, stream_ref, send_ref):
    mixed = dot(unpacked(all_ref), weight_ref[...])
    stream = (resid_ref[...].astype(F32) + mixed).astype(BF16)
    stream_ref[...] = stream
    send_ref[...] = dot(place_ref[...], stream).astype(BF16)


def spread_kernel(arrived_ref, keep_ref, send_ref):
    tokens = dot(keep_ref[...], arrived_ref[...]).astype(BF16)
    for t in range(send_ref.shape[0]):
        send_ref[t] = tokens


def inverse_of(tokens_ref):
    peers, rows, cols = tokens_ref.shape
    square = jnp.zeros((rows, cols), F32)
    for t in range(peers):
        part = tokens_ref[t].astype(F32)
        square = square + part * part
    return lax.rsqrt(jnp.sum(square, axis=1, keepdims=True) / (peers * cols) + EPSILON)


def expert_kernel(tokens_ref, gain_ref, gate_ref, up_ref, down_ref, out_ref):
    peers, rows, cols = tokens_ref.shape
    inverse = inverse_of(tokens_ref)
    normed = jnp.concatenate(
        [(tokens_ref[t].astype(F32) * inverse * gain_ref[t : t + 1, :]).astype(BF16) for t in range(peers)], axis=1
    )
    gate = jnp.minimum(dot(normed, gate_ref[0]), LIMIT)
    up = jnp.clip(dot(normed, up_ref[0]), -LIMIT, LIMIT)
    active = ((up + 1.0) * (gate * jax.nn.sigmoid(ALPHA * gate))).astype(BF16)
    for t in range(0, peers, 2):
        part = dot(active, down_ref[0, :, t * cols : (t + 2) * cols]).astype(BF16)
        out_ref[t] = part[:, :cols]
        out_ref[t + 1] = part[:, cols:]


def logit_kernel(tokens_ref, gain_ref, router_ref, tag_ref, out_ref):
    peers, rows, cols = tokens_ref.shape
    inverse = inverse_of(tokens_ref)
    total = jnp.zeros((rows, cols), F32)
    for t in range(peers):
        total = total + tokens_ref[t].astype(F32) * gain_ref[t : t + 1, :] * router_ref[t : t + 1, :]
    logit = jnp.sum(total, axis=1, keepdims=True) * inverse
    high, low = halves(logit)
    row = lax.broadcasted_iota(jnp.int32, (rows, TILE), 0)
    place = row - 9 * ninth(row)
    lane = lax.broadcasted_iota(jnp.int32, (rows, TILE), 1)
    marked = jnp.where(lane == place, high.astype(F32), 0.0) + jnp.where(lane == place + 16, low.astype(F32), 0.0)
    out_ref[...] = dot(tag_ref[...], marked.astype(BF16)).astype(BF16)


def return_kernel(parts_ref, grow_ref, logits_ref, send_ref):
    total = parts_ref[0].astype(F32)
    for t in range(1, parts_ref.shape[0]):
        total = total + parts_ref[t].astype(F32)
    grown = dot(grow_ref[...], total.astype(BF16))
    send_ref[...] = (grown + logits_ref[...].astype(F32)).astype(BF16)


def combine_kernel(top, back_ref, fetch_ref, pick_ref, stream_ref, out_ref):
    fetched = dot(fetch_ref[...], back_ref[...])
    seqs = stream_ref.shape[0]
    half = top * seqs
    picked = jnp.sum(fetched[half:] * pick_ref[...], axis=1, keepdims=True)
    expon = jnp.exp(picked)
    values = [fetched[k * seqs : (k + 1) * seqs] for k in range(top)]
    shares = [expon[k * seqs : (k + 1) * seqs] for k in range(top)]
    total = functools.reduce(jnp.add, shares)
    mixed = functools.reduce(jnp.add, [(share / total) * value for share, value in zip(shares, values)])
    out_ref[...] = (stream_ref[...].astype(F32) + mixed).astype(BF16)


def per_device(
    residual, state_re, state_im, mix_gain, proj_in, decay_rate, frequency, log_step, input_re, input_im,
    read_re, read_im, skip_gain, glu_weight, out_proj, ffn_gain, router, gate_weight, up_weight, down_weight,
    route_ids,
):
    seqs, cols = residual.shape
    width = mix_gain.shape[0]
    peers = width // cols
    groups, entries = decay_rate.shape
    channels = skip_gain.shape[0]
    ep_size = lax.axis_size("ep")
    experts = router.shape[1]
    top = route_ids.shape[1]
    cap = seqs * top // experts + 1
    per = cap + 1
    slots = ep_size * per
    rows = ep_size * cap
    half = seqs // 2

    all_resid = exchange(jnp.broadcast_to(residual[None], (peers, seqs, cols)), TP)

    place, fetch, pick, keep, grow, tag = call(
        functools.partial(routing_kernel, per, cap, experts),
        (
            shape_of((slots, seqs), BF16), shape_of((2 * top * seqs, slots), BF16), shape_of((top * seqs, TILE), F32),
            shape_of((rows, slots), BF16), shape_of((slots, rows), BF16), shape_of((slots, rows), BF16),
        ),
        route_ids, route_ids.T,
    )
    abar_re, abar_im, bbar_re, bbar_im = discretise(
        decay_rate, frequency, log_step, input_re.transpose(0, 2, 1), input_im.transpose(0, 2, 1)
    )
    lanes = groups * entries
    new_re, new_im, mixer, mixer_send = call(
        mixer_kernel,
        (
            shape_of((seqs, lanes), F32), shape_of((seqs, lanes), F32), shape_of((seqs, channels), F32),
            shape_of((peers, half, 2 * channels), BF16),
        ),
        all_resid, mix_gain.reshape(peers, cols), proj_in.T,
        state_re.reshape(seqs, lanes), state_im.reshape(seqs, lanes),
        abar_re.reshape(1, lanes), abar_im.reshape(1, lanes),
        block_diagonal(bbar_re), block_diagonal(bbar_im), block_diagonal(read_re), block_diagonal(read_im),
        skip_gain.reshape(1, channels),
    )
    all_mixer = exchange(mixer_send, TP)
    gated_send = call(
        gate_kernel, shape_of((peers, half, 2 * channels), BF16), all_mixer, glu_weight.T, mixer
    )
    all_gated = exchange(gated_send, TP)
    stream, token_send = call(
        stream_kernel,
        (shape_of((seqs, cols), BF16), shape_of((slots, cols), BF16)),
        all_gated, out_proj, residual, place,
    )
    arrived = exchange(token_send.reshape(ep_size, per // 2, 2, cols), "ep").reshape(slots, cols)
    tokens_send = call(spread_kernel, shape_of((peers, rows, cols), BF16), arrived, keep)
    tokens = exchange(tokens_send, TP)
    gain = ffn_gain.reshape(peers, cols)
    parts = call(
        expert_kernel, shape_of((peers, rows, cols), BF16), tokens, gain, gate_weight, up_weight, down_weight, mib=24
    )
    own_parts = exchange(parts, TP)
    expert = lax.axis_index("ep")
    own_router = lax.dynamic_slice_in_dim(router.T, expert, 1, 0).reshape(peers, cols)
    logits = call(logit_kernel, shape_of((slots, cols), BF16), tokens, gain, own_router, tag)
    back_send = call(return_kernel, shape_of((slots, cols), BF16), own_parts, grow, logits)
    back = exchange(back_send.reshape(ep_size, per // 2, 2, cols), "ep").reshape(slots, cols)
    layer_out = call(
        functools.partial(combine_kernel, top), shape_of((seqs, cols), BF16), back, fetch, pick, stream
    )
    shape = (seqs, groups, entries)
    return (layer_out, new_re.reshape(shape), new_im.reshape(shape))


def solution(mesh):
    split = Mesh(mesh.devices.reshape(mesh.shape["ep"], 4, 4), ("ep", "tp_0", "tp_1"))
    in_specs = (
        P("ep", TP),
        P("ep", TP, None),
        P("ep", TP, None),
        P(),
        P(None, TP),
        P(TP, None),
        P(TP, None),
        P(TP),
        P(TP, None, None),
        P(TP, None, None),
        P(TP, None, None),
        P(TP, None, None),
        P(TP),
        P(None, TP),
        P(None, TP),
        P(),
        P(),
        P("ep", None, TP),
        P("ep", None, TP),
        P("ep", TP, None),
        P("ep", None),
    )
    out_specs = (P("ep", TP), P("ep", TP, None), P("ep", TP, None))
    return jax.shard_map(
        per_device, mesh=split, in_specs=in_specs, out_specs=out_specs, check_vma=False
    )
```

time: 188 us -> 140 us (0.74)
  blocking collectives: 86.4 us -> 62.6 us
  waiting for transfers between devices: 46.9 us -> 36.2 us
  Pallas kernels: 0 us -> 7.17 us
  matrix products: 6.81 us -> 0 us
  local copies, waits for them, and re-layouts: 14.6 us -> 7.89 us
  starting transfers between devices: 28.8 us -> 23 us
    psum x2 -> x0, blocking collectives: 24.1 us -> none  [one_axis_at_a_time(): return functools.reduce(lax.psum, axes, shard)]
    all_to_all x5 -> x4, waiting for transfers between devices: 46.9 us -> 36.2 us  [exchange(): return lax.all_to_all(blocks, axis, 0, 0, tiled=True)]
    pallas_call x0 -> x9, Pallas kernels: none -> 7.17 us  [call(): pl.pallas_call(body, out_shape=out, compiler_params=pltpu.CompilerParams(...]
    dot_general x11 -> x0, matrix products: 6.81 us -> none  [the longest x1 2.69 us: per_device(): jnp.einsum('esf,efd->esd', active, down_weight, preferred_element_type=jn...]
    all_to_all x5 -> x4, starting transfers between devices: 28.8 us -> 23 us  [exchange(): return lax.all_to_all(blocks, axis, 0, 0, tiled=True)]
    unnamed x54 -> x45, local copies, waits for them, and re-layouts: 6.71 us -> 2.79 us
    all_to_all x2 -> x3, blocking collectives: 62.4 us -> 62.6 us  [exchange(): return lax.all_to_all(blocks, axis, 0, 0, tiled=True)]
  transfers between devices with their start and end apart: 5 -> 4, of which waited for: 5 -> 4; matrix products, arithmetic and copies ran while one was open for 3% -> 4% of each run, Pallas kernels for 0% -> 1%
where the time goes in v1:
time: 140 us
  blocking collectives  62.6 us (45%)
  waiting for transfers between devices  36.2 us (26%)
  starting transfers between devices  23 us (16%)
  local copies, waits for them, and re-layouts  7.89 us (6%)
  Pallas kernels  7.17 us (5%)
  other arithmetic  1.92 us (1%)
    all_to_all x3, blocking collectives, exchange(): return lax.all_to_all(blocks, axis, 0, 0, tiled=True)  62.6 us
    all_to_all x4, waiting for transfers between devices, exchange(): return lax.all_to_all(blocks, axis, 0, 0, tiled=True)  36.2 us
    all_to_all x4, starting transfers between devices, exchange(): return lax.all_to_all(blocks, axis, 0, 0, tiled=True)  23 us
    pallas_call x9, Pallas kernels, call(): pl.pallas_call(body, out_shape=out, compiler_params=pltpu.CompilerParams(...  7.17 us
  transfers between devices with their start and end apart: 4, of which 4 were waited for; matrix products, arithmetic and copies ran while one was open for 4% of the time, Pallas kernels for 1%

profile of v1, /device:TPU:1, one launch (start us, length us, event | category | flops | bytes accessed | tf_op | source)
XLA Modules:
  0.0 139.7 jit_solution(3498514815864381354)
XLA Ops:
  0.6 0.0 copy-start
  0.6 0.0 copy-start.19
  0.7 0.0 copy-start.21
  0.7 0.0 copy-start.20
  0.7 1.5 %broadcast_in_dim.8 = bf16[16,64,128]{2,1,0:T(8,128)(2,1)} broadcast(bf16[64,128]{1,0:T(8,128)(2,1)} %resid_ref.1), dimensions={1,2} | broadcast | bytes 278528 | tf_op jit(solution)/shard_map/broadcast_in_dim | solution.py:281
  2.2 7.6 %all-to-all-start = ((bf16[16,64,128]{2,1,0:T(8,128)(2,1)}), bf16[16,64,128]{2,1,0:T(8,128)(2,1)S(1)}, u32[]{:S(2)}, u32[]{:S(2)}) async-start(bf16[16,64,128]{2,1,0:T(8,128)(2,1)} %broadcast_in_dim.8), calls=%async_computation | async-start | bytes 524288 | tf_op jit(solution)/shard_map/all_to_all | solution.py:47
  9.8 0.0 copy-start.9
  9.9 0.7 exp.6
  10.6 0.8 add_divide_fusion
  11.4 0.8 multiply_add_fusion
  12.2 0.1 maximum_select_fusion.input_re_ref
  12.3 0.1 reshape.69.abar_re_ref
  12.4 0.1 reshape.70.abar_im_ref
  12.5 1.0 reshape.67.state_re_ref
  13.5 0.1 reshape.68.state_im_ref
  13.7 0.2 maximum_select_fusion.3
  13.9 3.7 %all-to-all-done.resid_ref = bf16[16,64,128]{2,1,0:T(8,128)(2,1)S(1)} async-done(((bf16[16,64,128]{2,1,0:T(8,128)(2,1)}), bf16[16,64,128]{2,1,0:T(8,128)(2,1)S(1)}, u32[]{:S(2)}, u32[]{:S(2)}) %all-to-all-start) | async-done | bytes 262176 | tf_op jit(solution)/shard_map/all_to_all | solution.py:47
  17.5 0.8 shard_map.220
  18.3 0.0 copy-start.10
  18.3 0.6 copy-done.10
  18.9 9.6 %all_to_all.35.all_ref = bf16[16,32,128]{2,1,0:T(8,128)(2,1)S(1)} all-to-all(bf16[16,32,128]{2,1,0:T(8,128)(2,1)S(1)} %get-tuple-element.15), channel_id=1, replica_groups=mesh['ep'=32,'tp_0'=4,'tp_1'=4] {'tp_0','tp_1'}, dimensions={0} | all-to-all | bytes 262144 | tf_op jit(solution)/shard_map/all_to_all | solution.py:47
  28.6 1.0 shard_map.221
  29.6 3.5 %all-to-all-start.2 = ((bf16[16,32,128]{2,1,0:T(8,128)(2,1)}), bf16[16,32,128]{2,1,0:T(8,128)(2,1)S(1)}, u32[]{:S(2)}, u32[]{:S(2)}) async-start(bf16[16,32,128]{2,1,0:T(8,128)(2,1)} %shard_map.221), calls=%async_computation.2 | async-start | bytes 262144 | tf_op jit(solution)/shard_map/all_to_all | solution.py:47
  33.1 0.1 copy.24.route_ref
  33.2 0.8 shard_map.222
  34.0 5.9 %all-to-all-done.2.all_ref = bf16[16,32,128]{2,1,0:T(8,128)(2,1)S(1)} async-done(((bf16[16,32,128]{2,1,0:T(8,128)(2,1)}), bf16[16,32,128]{2,1,0:T(8,128)(2,1)S(1)}, u32[]{:S(2)}, u32[]{:S(2)}) %all-to-all-start.2) | async-done | bytes 131104 | tf_op jit(solution)/shard_map/all_to_all | solution.py:47
  39.9 0.4 shard_map.223
  40.3 0.0 copy-start.14
  40.3 33.1 %all_to_all.36 = bf16[32,5,2,128]{3,2,1,0:T(2,128)(2,1)S(1)} all-to-all(bf16[32,5,2,128]{3,2,1,0:T(2,128)(2,1)S(1)} %bitcast.23), channel_id=1, replica_groups=mesh['ep'=32,'tp_0'=4,'tp_1'=4] {'ep'}, dimensions={0} | all-to-all | bytes 163840 | tf_op jit(solution)/shard_map/all_to_all | solution.py:47
  73.4 0.3 shard_map.224
  73.6 0.0 copy-start.2
  73.6 0.0 copy-start.3
  73.6 0.0 copy-start.13
  73.7 19.8 %all_to_all.37.tokens_ref = bf16[16,288,128]{2,1,0:T(8,128)(2,1)S(1)} all-to-all(bf16[16,288,128]{2,1,0:T(8,128)(2,1)S(1)} %shard_map.224), channel_id=1, replica_groups=mesh['ep'=32,'tp_0'=4,'tp_1'=4] {'tp_0','tp_1'}, dimensions={0} | all-to-all | bytes 2359296 | tf_op jit(solution)/shard_map/all_to_all | solution.py:47
  93.5 1.4 %shard_map.225 = bf16[16,288,128]{2,1,0:T(8,128)(2,1)S(1)} custom-call(bf16[16,288,128]{2,1,0:T(8,128)(2,1)S(1)} %all_to_all.37.tokens_ref, f32[16,128]{1,0:T(8,128)S(1)} %bitcast.24, bf16[1,2048,256]{2,1,0:T(8,128)(2,1)S(1)} %copy-done.2, bf16[1,2048,256]{2,1,0:T(8,128)(2,1)S(1)} %copy-done.3, bf16[1,256,2048]{2,1,0:T(8,128)(2,1)S(1)} %copy-done.4), custom_call_target="tpu_custom_call" | custom-call | tf_op jit(solution)/shard_map/pallas_call | solution.py:21
  94.9 1.0 copy-done.1
  96.0 3.7 %all-to-all-start.5 = ((bf16[16,288,128]{2,1,0:T(8,128)(2,1)}), bf16[16,288,128]{2,1,0:T(8,128)(2,1)S(1)}, u32[]{:S(2)}, u32[]{:S(2)}) async-start(bf16[16,288,128]{2,1,0:T(8,128)(2,1)} %copy-done.1), calls=%async_computation.5 | async-start | bytes 2359296 | tf_op jit(solution)/shard_map/all_to_all | solution.py:47
  99.7 0.9 copy-done.8
  100.7 0.7 shard_map.226.logits_ref
  101.4 0.0 copy-start.11
  101.4 0.0 copy-start.15
  101.4 14.4 %all-to-all-done.5.parts_ref = bf16[16,288,128]{2,1,0:T(8,128)(2,1)S(1)} async-done(((bf16[16,288,128]{2,1,0:T(8,128)(2,1)}), bf16[16,288,128]{2,1,0:T(8,128)(2,1)S(1)}, u32[]{:S(2)}, u32[]{:S(2)}) %all-to-all-start.5) | async-done | bytes 1179680 | tf_op jit(solution)/shard_map/all_to_all | solution.py:47
  115.8 1.0 shard_map.227
  116.8 8.3 %all-to-all-start.6 = ((bf16[32,5,2,128]{3,2,1,0:T(2,128)(2,1)}), bf16[32,5,2,128]{3,2,1,0:T(2,128)(2,1)S(1)}, u32[]{:S(2)}, u32[]{:S(2)}) async-start(bf16[32,5,2,128]{3,2,1,0:T(2,128)(2,1)} %bitcast.15), calls=%async_computation.6 | async-start | bytes 163840 | tf_op jit(solution)/shard_map/all_to_all | solution.py:47
  125.0 0.8 reshape.82
  125.8 0.8 reshape.83
  126.6 12.2 %all-to-all-done.6 = bf16[32,5,2,128]{3,2,1,0:T(2,128)(2,1)S(1)} async-done(((bf16[32,5,2,128]{3,2,1,0:T(2,128)(2,1)}), bf16[32,5,2,128]{3,2,1,0:T(2,128)(2,1)S(1)}, u32[]{:S(2)}, u32[]{:S(2)}) %all-to-all-start.6) | async-done | bytes 81952 | tf_op jit(solution)/shard_map/all_to_all | solution.py:47
  138.8 1.0 shard_map.228
  (34 shorter events, 0.1 us)
Async XLA Ops:
  0.6 99.1 %copy-start = (f32[2048,32]{0,1:T(8,128)S(1)}, f32[2048,32]{0,1:T(8,128)}, u32[]{:S(2)}) copy-start(f32[2048,32]{0,1:T(8,128)} %param.37) | copy-start | bytes 786436
  0.6 12.9 %copy-start.19 = (f32[64,4,64]{2,1,0:T(4,128)S(1)}, f32[64,4,64]{2,1,0:T(4,128)}, u32[]{:S(2)}) copy-start(f32[64,4,64]{2,1,0:T(4,128)} %param.23) | copy-start | bytes 196612
  0.7 13.0 %copy-start.21 = (f32[4,16,64]{2,1,0:T(8,128)S(1)}, f32[4,16,64]{2,1,0:T(8,128)}, u32[]{:S(2)}) copy-start(f32[4,16,64]{2,1,0:T(8,128)} %param.31) | copy-start | bytes 49156
  0.7 13.0 %copy-start.20 = (f32[4,16,64]{2,1,0:T(8,128)S(1)}, f32[4,16,64]{2,1,0:T(8,128)}, u32[]{:S(2)}) copy-start(f32[4,16,64]{2,1,0:T(8,128)} %param.32) | copy-start | bytes 49156
  0.7 16.8 %copy-start.16 = (f32[2048]{0:T(1024)S(1)}, f32[2048]{0:T(1024)}, u32[]{:S(2)}) copy-start(f32[2048]{0:T(1024)} %param.24) | copy-start | bytes 24580
  0.7 16.8 %copy-start.5 = (bf16[2048,64]{0,1:T(8,128)(2,1)S(1)}, bf16[2048,64]{0,1:T(8,128)(2,1)}, u32[]{:S(2)}) copy-start(bf16[2048,64]{0,1:T(8,128)(2,1)} %param.25) | copy-start | bytes 786436
  0.7 16.8 %copy-start.18 = (f32[64]{0:T(128)S(1)}, f32[64]{0:T(128)}, u32[]{:S(2)}) copy-start(f32[64]{0:T(128)} %param.33) | copy-start | bytes 772
  2.2 15.3 %all-to-all-start = ((bf16[16,64,128]{2,1,0:T(8,128)(2,1)}), bf16[16,64,128]{2,1,0:T(8,128)(2,1)S(1)}, u32[]{:S(2)}, u32[]{:S(2)}) async-start(bf16[16,64,128]{2,1,0:T(8,128)(2,1)} %broadcast_in_dim.8), calls=%async_computation | async-start | bytes 524288 | tf_op jit(solution)/shard_map/all_to_all | solution.py:47
  9.8 18.8 %copy-start.9 = (bf16[1024,64]{0,1:T(8,128)(2,1)S(1)}, bf16[1024,64]{0,1:T(8,128)(2,1)}, u32[]{:S(2)}) copy-start(bf16[1024,64]{0,1:T(8,128)(2,1)} %param.34) | copy-start | bytes 393220
  13.5 19.6 %copy-start.17 = (s32[64,4]{0,1:T(4,128)S(1)}, s32[64,4]{0,1:T(4,128)}, u32[]{:S(2)}) copy-start(s32[64,4]{0,1:T(4,128)} %param.41) | copy-start | bytes 3076
  13.6 26.2 %copy-start.6 = (bf16[1024,128]{1,0:T(8,128)(2,1)S(1)}, bf16[1024,128]{1,0:T(8,128)(2,1)}, u32[]{:S(2)}) copy-start(bf16[1024,128]{1,0:T(8,128)(2,1)} %weight_ref.1) | copy-start | bytes 786436
  13.7 26.2 %copy-start.12 = (bf16[64,128]{1,0:T(8,128)(2,1)S(1)}, bf16[64,128]{1,0:T(8,128)(2,1)}, u32[]{:S(2)}) copy-start(bf16[64,128]{1,0:T(8,128)(2,1)} %resid_ref.1) | copy-start | bytes 49156
  18.3 0.6 copy-start.10
  29.6 10.3 %all-to-all-start.2 = ((bf16[16,32,128]{2,1,0:T(8,128)(2,1)}), bf16[16,32,128]{2,1,0:T(8,128)(2,1)S(1)}, u32[]{:S(2)}, u32[]{:S(2)}) async-start(bf16[16,32,128]{2,1,0:T(8,128)(2,1)} %shard_map.221), calls=%async_computation.2 | async-start | bytes 262144 | tf_op jit(solution)/shard_map/all_to_all | solution.py:47
  34.0 39.4 %copy-start.7 = (bf16[320,288]{1,0:T(8,128)(2,1)}, bf16[320,288]{1,0:T(8,128)(2,1)S(1)}, u32[]{:S(2)}) copy-start(bf16[320,288]{1,0:T(8,128)(2,1)S(1)} %get-tuple-element.21.tag_ref) | copy-start | bytes 552964
  40.3 53.2 %copy-start.14 = (bf16[64,128]{1,0:T(8,128)(2,1)}, bf16[64,128]{1,0:T(8,128)(2,1)S(1)}, u32[]{:S(2)}) copy-start(bf16[64,128]{1,0:T(8,128)(2,1)S(1)} %get-tuple-element.24.stream_ref) | copy-start | bytes 49156
  73.4 20.1 %copy-start.4 = (bf16[1,256,2048]{2,1,0:T(8,128)(2,1)S(1)}, bf16[1,256,2048]{2,1,0:T(8,128)(2,1)}, u32[]{:S(2)}) copy-start(bf16[1,256,2048]{2,1,0:T(8,128)(2,1)} %down_ref.1) | copy-start | bytes 3145732
  73.6 19.9 %copy-start.2 = (bf16[1,2048,256]{2,1,0:T(8,128)(2,1)S(1)}, bf16[1,2048,256]{2,1,0:T(8,128)(2,1)}, u32[]{:S(2)}) copy-start(bf16[1,2048,256]{2,1,0:T(8,128)(2,1)} %gate_ref.1) | copy-start | bytes 3145732
  73.6 19.9 %copy-start.3 = (bf16[1,2048,256]{2,1,0:T(8,128)(2,1)S(1)}, bf16[1,2048,256]{2,1,0:T(8,128)(2,1)}, u32[]{:S(2)}) copy-start(bf16[1,2048,256]{2,1,0:T(8,128)(2,1)} %up_ref.1) | copy-start | bytes 3145732
  73.6 19.9 %copy-start.13 = (f32[2048]{0:T(1024)S(1)}, f32[2048]{0:T(1024)}, u32[]{:S(2)}) copy-start(f32[2048]{0:T(1024)} %param.36) | copy-start | bytes 24580
  94.9 1.0 copy-start.1
  96.0 19.8 %all-to-all-start.5 = ((bf16[16,288,128]{2,1,0:T(8,128)(2,1)}), bf16[16,288,128]{2,1,0:T(8,128)(2,1)S(1)}, u32[]{:S(2)}, u32[]{:S(2)}) async-start(bf16[16,288,128]{2,1,0:T(8,128)(2,1)} %copy-done.1), calls=%async_computation.5 | async-start | bytes 2359296 | tf_op jit(solution)/shard_map/all_to_all | solution.py:47
  99.7 0.9 copy-start.8
  101.4 23.7 %copy-start.11 = (f32[64,256]{1,0:T(8,128)S(1)}, f32[64,256]{1,0:T(8,128)}, u32[]{:S(2)}) copy-start(f32[64,256]{1,0:T(8,128)} %copy-done.10) | copy-start | bytes 196612
  101.4 37.4 %copy-start.15 = (bf16[64,128]{1,0:T(8,128)(2,1)S(1)}, bf16[64,128]{1,0:T(8,128)(2,1)}, u32[]{:S(2)}) copy-start(bf16[64,128]{1,0:T(8,128)(2,1)} %copy-done.14) | copy-start | bytes 49156
  116.8 22.0 %all-to-all-start.6 = ((bf16[32,5,2,128]{3,2,1,0:T(2,128)(2,1)}), bf16[32,5,2,128]{3,2,1,0:T(2,128)(2,1)S(1)}, u32[]{:S(2)}, u32[]{:S(2)}) async-start(bf16[32,5,2,128]{3,2,1,0:T(2,128)(2,1)} %bitcast.15), calls=%async_computation.6 | async-start | bytes 163840 | tf_op jit(solution)/shard_map/all_to_all | solution.py:47

commit v2 on v1

--- a/solution.py
+++ b/solution.py
@@ -15,6 +15,7 @@
 F32 = jnp.float32
 BF16 = jnp.bfloat16
 TILE = 128
+STAGGER = 9000
 
 
 def call(body, out, *args, mib=16, **settings):
@@ -64,10 +65,10 @@
 
 def block_diagonal(blocks):
     count, rows, cols = blocks.shape
-    flat = blocks.reshape(count * rows, cols)
+    flat = jnp.pad(blocks.reshape(count * rows, cols), ((0, 0), (0, TILE - cols)))
     wide = jnp.concatenate([flat] * count, axis=1)
     row_block = lax.broadcasted_iota(jnp.int32, wide.shape, 0) // rows
-    col_block = lax.broadcasted_iota(jnp.int32, wide.shape, 1) // cols
+    col_block = lax.broadcasted_iota(jnp.int32, wide.shape, 1) // TILE
     return jnp.where(row_block == col_block, wide, 0.0)
 
 
@@ -90,7 +91,7 @@
     return jnp.concatenate(rows, axis=0).astype(BF16)
 
 
-def routing_kernel(per, cap, experts, route_ref, across_ref, place_ref, fetch_ref, pick_ref, keep_ref, grow_ref, tag_ref):
+def routing_kernel(per, cap, experts, route_ref, across_ref, place_ref, fetch_ref, pick_ref, keep_ref, grow_ref):
     seqs, top = route_ref.shape
     slots = place_ref.shape[0]
     rows = keep_ref.shape[0]
@@ -129,8 +130,9 @@
     row = iota((rows, slots), 0)
     keep_ref[...] = (iota((rows, slots), 1) == row + ninth(row)).astype(F32).astype(BF16)
     col = iota((slots, rows), 1)
-    grow_ref[...] = (iota((slots, rows), 0) == col + ninth(col)).astype(F32).astype(BF16)
-    tag_ref[...] = (iota((slots, rows), 0) == ninth(col) * per + cap).astype(F32).astype(BF16)
+    target = iota((slots, rows), 0)
+    grow_ref[0] = (target == col + ninth(col)).astype(F32).astype(BF16)
+    grow_ref[1] = (target == ninth(col) * per + cap).astype(F32).astype(BF16)
 
 
 def ninth(value):
@@ -143,6 +145,7 @@
     new_re_ref, new_im_ref, mixer_ref, send_ref,
 ):
     peers, seqs, cols = resid_ref.shape
+    groups, entries = abar_re_ref.shape
     square = jnp.zeros((seqs, cols), F32)
     for t in range(peers):
         part = resid_ref[t].astype(F32)
@@ -153,25 +156,31 @@
         [(resid_ref[t].astype(F32) * scale * gain_ref[t : t + 1, :]).astype(BF16) for t in range(peers)], axis=1
     )
     mix = dot_rows(normed, proj_ref[...]).astype(BF16)
-    width = state_re_ref.shape[1]
 
     def driven(ref):
         high, low = halves(ref[...])
         return dot(mix, high) + dot(mix, low)
 
-    old_re, old_im = state_re_ref[...], state_im_ref[...]
-    abar_re, abar_im = abar_re_ref[...], abar_im_ref[...]
-    new_re = abar_re * old_re - abar_im * old_im + driven(input_re_ref)
-    new_im = abar_re * old_im + abar_im * old_re + driven(input_im_ref)
-    new_re_ref[...] = new_re
-    new_im_ref[...] = new_im
-
-    def read(value, ref):
-        high, low = halves(value)
+    drive_re, drive_im = driven(input_re_ref), driven(input_im_ref)
+    pad = jnp.zeros((seqs, TILE - entries), F32)
+    all_re, all_im = [], []
+    for g in range(groups):
+        old_re, old_im = state_re_ref[:, g, :], state_im_ref[:, g, :]
+        abar_re, abar_im = abar_re_ref[g : g + 1, :], abar_im_ref[g : g + 1, :]
+        own = slice(g * TILE, g * TILE + entries)
+        new_re = abar_re * old_re - abar_im * old_im + drive_re[:, own]
+        new_im = abar_re * old_im + abar_im * old_re + drive_im[:, own]
+        new_re_ref[:, g, :] = new_re
+        new_im_ref[:, g, :] = new_im
+        all_re += [new_re, pad]
+        all_im += [new_im, pad]
+
+    def read(values, ref):
+        high, low = halves(jnp.concatenate(values, axis=1))
         read_high, read_low = halves(ref[...])
         return dot_rows(high, read_high) + dot_rows(high, read_low) + dot_rows(low, read_high)
 
-    value = read(new_re, read_re_ref) - read(new_im, read_im_ref) + skip_ref[...] * mix.astype(F32)
+    value = read(all_re, read_re_ref) - read(all_im, read_im_ref) + skip_ref[...] * mix.astype(F32)
     mixer = 0.5 * value * (1.0 + lax.erf(value * 0.7071067811865476))
     mixer_ref[...] = mixer
     sent = packed(mixer).astype(BF16)
@@ -197,20 +206,27 @@
     tokens = dot(keep_ref[...], arrived_ref[...]).astype(BF16)
     for t in range(send_ref.shape[0]):
         send_ref[t] = tokens
-
-
-def inverse_of(tokens_ref):
+    if STAGGER:
+        @pl.when(lax.rem(lax.axis_index("ep"), 2) == 1)
+        def _():
+            pl.delay(STAGGER)
+
+
+def expert_kernel(tokens_ref, gain_ref, router_ref, gate_ref, up_ref, down_ref, out_ref, logit_ref):
     peers, rows, cols = tokens_ref.shape
     square = jnp.zeros((rows, cols), F32)
+    total = jnp.zeros((rows, cols), F32)
     for t in range(peers):
         part = tokens_ref[t].astype(F32)
         square = square + part * part
-    return lax.rsqrt(jnp.sum(square, axis=1, keepdims=True) / (peers * cols) + EPSILON)
-
-
-def expert_kernel(tokens_ref, gain_ref, gate_ref, up_ref, down_ref, out_ref):
-    peers, rows, cols = tokens_ref.shape
-    inverse = inverse_of(tokens_ref)
+        total = total + part * gain_ref[t : t + 1, :] * router_ref[t : t + 1, :]
+    inverse = lax.rsqrt(jnp.sum(square, axis=1, keepdims=True) / (peers * cols) + EPSILON)
+    high, low = halves(jnp.sum(total, axis=1, keepdims=True) * inverse)
+    row = lax.broadcasted_iota(jnp.int32, (rows, TILE), 0)
+    place = row - 9 * ninth(row)
+    lane = lax.broadcasted_iota(jnp.int32, (rows, TILE), 1)
+    marked = jnp.where(lane == place, high.astype(F32), 0.0) + jnp.where(lane == place + 16, low.astype(F32), 0.0)
+    logit_ref[...] = marked.astype(BF16)
     normed = jnp.concatenate(
         [(tokens_ref[t].astype(F32) * inverse * gain_ref[t : t + 1, :]).astype(BF16) for t in range(peers)], axis=1
     )
@@ -223,27 +239,12 @@
         out_ref[t + 1] = part[:, cols:]
 
 
-def logit_kernel(tokens_ref, gain_ref, router_ref, tag_ref, out_ref):
-    peers, rows, cols = tokens_ref.shape
-    inverse = inverse_of(tokens_ref)
-    total = jnp.zeros((rows, cols), F32)
-    for t in range(peers):
-        total = total + tokens_ref[t].astype(F32) * gain_ref[t : t + 1, :] * router_ref[t : t + 1, :]
-    logit = jnp.sum(total, axis=1, keepdims=True) * inverse
-    high, low = halves(logit)
-    row = lax.broadcasted_iota(jnp.int32, (rows, TILE), 0)
-    place = row - 9 * ninth(row)
-    lane = lax.broadcasted_iota(jnp.int32, (rows, TILE), 1)
-    marked = jnp.where(lane == place, high.astype(F32), 0.0) + jnp.where(lane == place + 16, low.astype(F32), 0.0)
-    out_ref[...] = dot(tag_ref[...], marked.astype(BF16)).astype(BF16)
-
-
 def return_kernel(parts_ref, grow_ref, logits_ref, send_ref):
     total = parts_ref[0].astype(F32)
     for t in range(1, parts_ref.shape[0]):
         total = total + parts_ref[t].astype(F32)
-    grown = dot(grow_ref[...], total.astype(BF16))
-    send_ref[...] = (grown + logits_ref[...].astype(F32)).astype(BF16)
+    grown = dot(grow_ref[0], total.astype(BF16)) + dot(grow_ref[1], logits_ref[...])
+    send_ref[...] = grown.astype(BF16)
 
 
 def combine_kernel(top, back_ref, fetch_ref, pick_ref, stream_ref, out_ref):
@@ -267,7 +268,6 @@
     seqs, cols = residual.shape
     width = mix_gain.shape[0]
     peers = width // cols
-    groups, entries = decay_rate.shape
     channels = skip_gain.shape[0]
     ep_size = lax.axis_size("ep")
     experts = router.shape[1]
@@ -280,27 +280,30 @@
 
     all_resid = exchange(jnp.broadcast_to(residual[None], (peers, seqs, cols)), TP)
 
-    place, fetch, pick, keep, grow, tag = call(
+    place, fetch, pick, keep, grow = call(
         functools.partial(routing_kernel, per, cap, experts),
         (
             shape_of((slots, seqs), BF16), shape_of((2 * top * seqs, slots), BF16), shape_of((top * seqs, TILE), F32),
-            shape_of((rows, slots), BF16), shape_of((slots, rows), BF16), shape_of((slots, rows), BF16),
+            shape_of((rows, slots), BF16), shape_of((2, slots, rows), BF16),
         ),
         route_ids, route_ids.T,
     )
     abar_re, abar_im, bbar_re, bbar_im = discretise(
         decay_rate, frequency, log_step, input_re.transpose(0, 2, 1), input_im.transpose(0, 2, 1)
     )
-    lanes = groups * entries
+    expert = lax.axis_index("ep")
+    own_router = lax.dynamic_slice_in_dim(router.T, expert, 1, 0).reshape(peers, cols)
+    gain = ffn_gain.reshape(peers, cols)
+    all_resid, place, fetch, pick, keep, grow, own_router, gain = lax.optimization_barrier(
+        (all_resid, place, fetch, pick, keep, grow, own_router, gain)
+    )
     new_re, new_im, mixer, mixer_send = call(
         mixer_kernel,
         (
-            shape_of((seqs, lanes), F32), shape_of((seqs, lanes), F32), shape_of((seqs, channels), F32),
+            shape_of(state_re.shape, F32), shape_of(state_im.shape, F32), shape_of((seqs, channels), F32),
             shape_of((peers, half, 2 * channels), BF16),
         ),
-        all_resid, mix_gain.reshape(peers, cols), proj_in.T,
-        state_re.reshape(seqs, lanes), state_im.reshape(seqs, lanes),
-        abar_re.reshape(1, lanes), abar_im.reshape(1, lanes),
+        all_resid, mix_gain.reshape(peers, cols), proj_in.T, state_re, state_im, abar_re, abar_im,
         block_diagonal(bbar_re), block_diagonal(bbar_im), block_diagonal(read_re), block_diagonal(read_im),
         skip_gain.reshape(1, channels),
     )
@@ -317,21 +320,17 @@
     arrived = exchange(token_send.reshape(ep_size, per // 2, 2, cols), "ep").reshape(slots, cols)
     tokens_send = call(spread_kernel, shape_of((peers, rows, cols), BF16), arrived, keep)
     tokens = exchange(tokens_send, TP)
-    gain = ffn_gain.reshape(peers, cols)
-    parts = call(
-        expert_kernel, shape_of((peers, rows, cols), BF16), tokens, gain, gate_weight, up_weight, down_weight, mib=24
+    parts, logits = call(
+        expert_kernel, (shape_of((peers, rows, cols), BF16), shape_of((rows, TILE), BF16)),
+        tokens, gain, own_router, gate_weight, up_weight, down_weight, mib=24,
     )
     own_parts = exchange(parts, TP)
-    expert = lax.axis_index("ep")
-    own_router = lax.dynamic_slice_in_dim(router.T, expert, 1, 0).reshape(peers, cols)
-    logits = call(logit_kernel, shape_of((slots, cols), BF16), tokens, gain, own_router, tag)
     back_send = call(return_kernel, shape_of((slots, cols), BF16), own_parts, grow, logits)
     back = exchange(back_send.reshape(ep_size, per // 2, 2, cols), "ep").reshape(slots, cols)
     layer_out = call(
         functools.partial(combine_kernel, top), shape_of((seqs, cols), BF16), back, fetch, pick, stream
     )
-    shape = (seqs, groups, entries)
-    return (layer_out, new_re.reshape(shape), new_im.reshape(shape))
+    return (layer_out, new_re, new_im)
 
 
 def solution(mesh):

time: 140 us -> 133 us (0.950)
  blocking collectives: 62.6 us -> 109 us
  waiting for transfers between devices: 36.2 us -> 4.14 us
  starting transfers between devices: 23 us -> 7.57 us
  local copies, waits for them, and re-layouts: 7.89 us -> 2.44 us
    all_to_all x3 -> x6, blocking collectives: 62.6 us -> 109 us  [exchange(): return lax.all_to_all(blocks, axis, 0, 0, tiled=True)]
    all_to_all x4 -> x1, waiting for transfers between devices: 36.2 us -> 4.14 us  [exchange(): return lax.all_to_all(blocks, axis, 0, 0, tiled=True)]
    all_to_all x4 -> x1, starting transfers between devices: 23 us -> 7.57 us  [exchange(): return lax.all_to_all(blocks, axis, 0, 0, tiled=True)]
    reshape x6 -> x0, local copies, waits for them, and re-layouts: 2.87 us -> none  [the longest x2 1.53 us: per_device(): return (layer_out, new_re.reshape(shape), new_im.reshape(shape))]
    unnamed x45 -> x33, local copies, waits for them, and re-layouts: 2.79 us -> 0.18 us
    pallas_call x9 -> x8, Pallas kernels: 7.17 us -> 6.16 us  [call(): pl.pallas_call(body, out_shape=out, compiler_params=pltpu.CompilerParams(...]
  transfers between devices with their start and end apart: 4 -> 1, of which waited for: 4 -> 1; matrix products, arithmetic and copies ran while one was open for 4% -> 2% of each run, Pallas kernels for 1% -> 1%
where the time goes in v2:
time: 133 us; the launch traced here: 132 us
  blocking collectives  109 us (82%)
  starting transfers between devices  7.57 us (6%)
  Pallas kernels  6.16 us (5%)
  waiting for transfers between devices  4.14 us (3%)
  local copies, waits for them, and re-layouts  2.44 us (2%)
  other arithmetic  1.83 us (1%)
    all_to_all x6, blocking collectives, exchange(): return lax.all_to_all(blocks, axis, 0, 0, tiled=True)  109 us
    all_to_all x1, starting transfers between devices, exchange(): return lax.all_to_all(blocks, axis, 0, 0, tiled=True)  7.57 us
    pallas_call x8, Pallas kernels, call(): pl.pallas_call(body, out_shape=out, compiler_params=pltpu.CompilerParams(...  6.16 us
    all_to_all x1, waiting for transfers between devices, exchange(): return lax.all_to_all(blocks, axis, 0, 0, tiled=True)  4.14 us
  transfers between devices with their start and end apart: 1, of which 1 were waited for; matrix products, arithmetic and copies ran while one was open for 2% of the time, Pallas kernels for 1%

profile of v2, /device:TPU:1, one launch (start us, length us, event | category | flops | bytes accessed | tf_op | source)
XLA Modules:
  0.0 132.5 jit_solution(2504053200667577234)
XLA Ops:
  0.6 0.0 copy-start
  0.6 0.0 copy-start.14
  0.7 0.0 copy-start.15
  0.7 0.0 copy-start.12
  0.7 0.0 copy-start.13
  0.7 0.0 copy-start.4
  0.7 0.0 copy-start.10
  0.7 0.0 copy-start.7
  0.7 0.0 copy-start.6
  0.7 1.6 %broadcast_in_dim.8 = bf16[16,64,128]{2,1,0:T(8,128)(2,1)} broadcast(bf16[64,128]{1,0:T(8,128)(2,1)} %resid_ref.1), dimensions={1,2} | broadcast | bytes 278528 | tf_op jit(solution)/shard_map/broadcast_in_dim | solution.py:281
  2.3 7.6 %all-to-all-start = ((bf16[16,64,128]{2,1,0:T(8,128)(2,1)}), bf16[16,64,128]{2,1,0:T(8,128)(2,1)S(1)}, u32[]{:S(2)}, u32[]{:S(2)}) async-start(bf16[16,64,128]{2,1,0:T(8,128)(2,1)} %broadcast_in_dim.8), calls=%async_computation | async-start | bytes 524288 | tf_op jit(solution)/shard_map/all_to_all | solution.py:48
  9.9 0.7 exp.6
  10.6 0.8 add_divide_fusion
  11.4 0.8 multiply_add_fusion
  12.2 0.1 maximum_select_fusion.input_re_ref
  12.3 0.0 copy-done
  12.3 0.0 copy-done.14
  12.4 0.0 copy-start.8
  12.4 0.0 copy-done.15
  12.4 0.0 copy-done.12
  12.4 0.1 copy.24.route_ref
  12.5 0.8 shard_map.220
  13.3 0.1 maximum_select_fusion.3
  13.4 0.0 copy-start.5
  13.4 0.0 copy-start.9
  13.4 4.1 %all-to-all-done.resid_ref = bf16[16,64,128]{2,1,0:T(8,128)(2,1)S(1)} async-done(((bf16[16,64,128]{2,1,0:T(8,128)(2,1)}), bf16[16,64,128]{2,1,0:T(8,128)(2,1)S(1)}, u32[]{:S(2)}, u32[]{:S(2)}) %all-to-all-start) | async-done | bytes 262176 | tf_op jit(solution)/shard_map/all_to_all | solution.py:48
  17.6 0.0 copy-done.13
  17.6 0.0 copy-done.4
  17.6 0.0 copy-done.10
  17.6 0.0 copy-done.7
  17.6 0.0 copy-done.6
  17.6 1.4 %shard_map.221 = (f32[64,4,64]{2,1,0:T(4,128)}, f32[64,4,64]{2,1,0:T(4,128)}, f32[64,64]{1,0:T(8,128)S(1)}, bf16[16,32,128]{2,1,0:T(8,128)(2,1)S(1)}) custom-call(bf16[16,64,128]{2,1,0:T(8,128)(2,1)S(1)} %all-to-all-done.resid_ref, f32[16,128]{1,0:T(8,128)S(1)} %bitcast.26, bf16[64,2048]{1,0:T(8,128)(2,1)S(1)} %bitcast.22, f32[64,4,64]{2,1,0:T(4,128)S(1)} %copy-done.6, ...), custom_call_target="tpu_custom_call" | custom-call | tf_op jit(solution)/shard_map/pallas_call | solution.py:22
  19.0 9.6 %all_to_all.35.all_ref = bf16[16,32,128]{2,1,0:T(8,128)(2,1)S(1)} all-to-all(bf16[16,32,128]{2,1,0:T(8,128)(2,1)S(1)} %get-tuple-element.30), channel_id=1, replica_groups=mesh['ep'=32,'tp_0'=4,'tp_1'=4] {'tp_0','tp_1'}, dimensions={0} | all-to-all | bytes 262144 | tf_op jit(solution)/shard_map/all_to_all | solution.py:48
  28.6 0.3 shard_map.222
  28.9 9.6 %all_to_all.36.all_ref = bf16[16,32,128]{2,1,0:T(8,128)(2,1)S(1)} all-to-all(bf16[16,32,128]{2,1,0:T(8,128)(2,1)S(1)} %shard_map.222), channel_id=1, replica_groups=mesh['ep'=32,'tp_0'=4,'tp_1'=4] {'tp_0','tp_1'}, dimensions={0} | all-to-all | bytes 262144 | tf_op jit(solution)/shard_map/all_to_all | solution.py:48
  38.6 0.4 shard_map.223
  39.0 33.4 %all_to_all.37 = bf16[32,5,2,128]{3,2,1,0:T(2,128)(2,1)S(1)} all-to-all(bf16[32,5,2,128]{3,2,1,0:T(2,128)(2,1)S(1)} %bitcast.24), channel_id=1, replica_groups=mesh['ep'=32,'tp_0'=4,'tp_1'=4] {'ep'}, dimensions={0} | all-to-all | bytes 163840 | tf_op jit(solution)/shard_map/all_to_all | solution.py:48
  72.4 0.3 shard_map.224
  72.7 0.0 copy-start.1
  72.7 0.0 copy-start.2
  72.7 0.0 copy-start.11
  72.7 24.4 %all_to_all.38.tokens_ref = bf16[16,288,128]{2,1,0:T(8,128)(2,1)S(1)} all-to-all(bf16[16,288,128]{2,1,0:T(8,128)(2,1)S(1)} %shard_map.224), channel_id=1, replica_groups=mesh['ep'=32,'tp_0'=4,'tp_1'=4] {'tp_0','tp_1'}, dimensions={0} | all-to-all | bytes 2359296 | tf_op jit(solution)/shard_map/all_to_all | solution.py:48
  97.1 0.0 copy-done.1
  97.1 1.7 %shard_map.225 = (bf16[16,288,128]{2,1,0:T(8,128)(2,1)S(1)}, bf16[288,128]{1,0:T(8,128)(2,1)S(1)}) custom-call(bf16[16,288,128]{2,1,0:T(8,128)(2,1)S(1)} %all_to_all.38.tokens_ref, f32[16,128]{1,0:T(8,128)S(1)} %bitcast.27, f32[16,128]{1,0:T(8,128)S(1)} %bitcast.25, bf16[1,2048,256]{2,1,0:T(8,128)(2,1)S(1)} %copy-done.1, ...), custom_call_target="tpu_custom_call" | custom-call | tf_op jit(solution)/shard_map/pallas_call | solution.py:22
  98.8 16.7 %all_to_all.39.parts_ref = bf16[16,288,128]{2,1,0:T(8,128)(2,1)S(1)} all-to-all(bf16[16,288,128]{2,1,0:T(8,128)(2,1)S(1)} %get-tuple-element.37), channel_id=1, replica_groups=mesh['ep'=32,'tp_0'=4,'tp_1'=4] {'tp_0','tp_1'}, dimensions={0} | all-to-all | bytes 2359296 | tf_op jit(solution)/shard_map/all_to_all | solution.py:48
  115.4 0.4 shard_map.226
  115.8 15.7 %all_to_all.40 = bf16[32,5,2,128]{3,2,1,0:T(2,128)(2,1)S(1)} all-to-all(bf16[32,5,2,128]{3,2,1,0:T(2,128)(2,1)S(1)} %bitcast.19), channel_id=1, replica_groups=mesh['ep'=32,'tp_0'=4,'tp_1'=4] {'ep'}, dimensions={0} | all-to-all | bytes 163840 | tf_op jit(solution)/shard_map/all_to_all | solution.py:48
  131.5 1.0 shard_map.227
  (16 shorter events, 0.1 us)
Async XLA Ops:
  0.6 11.7 %copy-start = (f32[2048,32]{0,1:T(8,128)S(1)}, f32[2048,32]{0,1:T(8,128)}, u32[]{:S(2)}) copy-start(f32[2048,32]{0,1:T(8,128)} %param.37) | copy-start | bytes 786436
  0.6 11.7 %copy-start.14 = (f32[4,16,64]{2,1,0:T(8,128)S(1)}, f32[4,16,64]{2,1,0:T(8,128)}, u32[]{:S(2)}) copy-start(f32[4,16,64]{2,1,0:T(8,128)} %param.31) | copy-start | bytes 49156
  0.7 11.7 %copy-start.15 = (f32[4,16,64]{2,1,0:T(8,128)S(1)}, f32[4,16,64]{2,1,0:T(8,128)}, u32[]{:S(2)}) copy-start(f32[4,16,64]{2,1,0:T(8,128)} %param.32) | copy-start | bytes 49156
  0.7 11.7 %copy-start.12 = (s32[64,4]{0,1:T(4,128)S(1)}, s32[64,4]{0,1:T(4,128)}, u32[]{:S(2)}) copy-start(s32[64,4]{0,1:T(4,128)} %param.41) | copy-start | bytes 3076
  0.7 16.9 %copy-start.13 = (f32[64]{0:T(128)S(1)}, f32[64]{0:T(128)}, u32[]{:S(2)}) copy-start(f32[64]{0:T(128)} %param.33) | copy-start | bytes 772
  0.7 16.9 %copy-start.4 = (bf16[2048,64]{0,1:T(8,128)(2,1)S(1)}, bf16[2048,64]{0,1:T(8,128)(2,1)}, u32[]{:S(2)}) copy-start(bf16[2048,64]{0,1:T(8,128)(2,1)} %param.25) | copy-start | bytes 786436
  0.7 16.9 %copy-start.10 = (f32[2048]{0:T(1024)S(1)}, f32[2048]{0:T(1024)}, u32[]{:S(2)}) copy-start(f32[2048]{0:T(1024)} %param.24) | copy-start | bytes 24580
  0.7 16.9 %copy-start.7 = (f32[64,4,64]{2,1,0:T(4,128)S(1)}, f32[64,4,64]{2,1,0:T(4,128)}, u32[]{:S(2)}) copy-start(f32[64,4,64]{2,1,0:T(4,128)} %state_im_ref.1) | copy-start | bytes 196612
  0.7 16.9 %copy-start.6 = (f32[64,4,64]{2,1,0:T(4,128)S(1)}, f32[64,4,64]{2,1,0:T(4,128)}, u32[]{:S(2)}) copy-start(f32[64,4,64]{2,1,0:T(4,128)} %state_re_ref.1) | copy-start | bytes 196612
  2.3 15.3 %all-to-all-start = ((bf16[16,64,128]{2,1,0:T(8,128)(2,1)}), bf16[16,64,128]{2,1,0:T(8,128)(2,1)S(1)}, u32[]{:S(2)}, u32[]{:S(2)}) async-start(bf16[16,64,128]{2,1,0:T(8,128)(2,1)} %broadcast_in_dim.8), calls=%async_computation | async-start | bytes 524288 | tf_op jit(solution)/shard_map/all_to_all | solution.py:48
  12.4 16.3 %copy-start.8 = (bf16[1024,64]{0,1:T(8,128)(2,1)S(1)}, bf16[1024,64]{0,1:T(8,128)(2,1)}, u32[]{:S(2)}) copy-start(bf16[1024,64]{0,1:T(8,128)(2,1)} %param.34) | copy-start | bytes 393220
  13.4 25.2 %copy-start.5 = (bf16[1024,128]{1,0:T(8,128)(2,1)S(1)}, bf16[1024,128]{1,0:T(8,128)(2,1)}, u32[]{:S(2)}) copy-start(bf16[1024,128]{1,0:T(8,128)(2,1)} %weight_ref.1) | copy-start | bytes 786436
  13.4 25.2 %copy-start.9 = (bf16[64,128]{1,0:T(8,128)(2,1)S(1)}, bf16[64,128]{1,0:T(8,128)(2,1)}, u32[]{:S(2)}) copy-start(bf16[64,128]{1,0:T(8,128)(2,1)} %resid_ref.1) | copy-start | bytes 49156
  72.4 24.7 %copy-start.3 = (bf16[1,256,2048]{2,1,0:T(8,128)(2,1)S(1)}, bf16[1,256,2048]{2,1,0:T(8,128)(2,1)}, u32[]{:S(2)}) copy-start(bf16[1,256,2048]{2,1,0:T(8,128)(2,1)} %down_ref.1) | copy-start | bytes 3145732
  72.7 24.4 %copy-start.1 = (bf16[1,2048,256]{2,1,0:T(8,128)(2,1)S(1)}, bf16[1,2048,256]{2,1,0:T(8,128)(2,1)}, u32[]{:S(2)}) copy-start(bf16[1,2048,256]{2,1,0:T(8,128)(2,1)} %gate_ref.1) | copy-start | bytes 3145732
  72.7 24.4 %copy-start.2 = (bf16[1,2048,256]{2,1,0:T(8,128)(2,1)S(1)}, bf16[1,2048,256]{2,1,0:T(8,128)(2,1)}, u32[]{:S(2)}) copy-start(bf16[1,2048,256]{2,1,0:T(8,128)(2,1)} %up_ref.1) | copy-start | bytes 3145732
  72.7 24.4 %copy-start.11 = (f32[2048]{0:T(1024)S(1)}, f32[2048]{0:T(1024)}, u32[]{:S(2)}) copy-start(f32[2048]{0:T(1024)} %param.36) | copy-start | bytes 24580

commit v3 on v2

--- a/solution.py
+++ b/solution.py
@@ -212,14 +212,23 @@
             pl.delay(STAGGER)
 
 
-def expert_kernel(tokens_ref, gain_ref, router_ref, gate_ref, up_ref, down_ref, out_ref, logit_ref):
+def expert_kernel(
+    tokens_ref, gain_ref, router_ref, gate_ref, up_ref, down_ref, new_re_ref, new_im_ref,
+    out_ref, logit_ref, out_re_ref, out_im_ref, sems,
+):
     peers, rows, cols = tokens_ref.shape
+    copies = [
+        pltpu.make_async_copy(new_re_ref, out_re_ref, sems.at[0]),
+        pltpu.make_async_copy(new_im_ref, out_im_ref, sems.at[1]),
+    ]
+    for copy in copies:
+        copy.start()
     square = jnp.zeros((rows, cols), F32)
     total = jnp.zeros((rows, cols), F32)
     for t in range(peers):
         part = tokens_ref[t].astype(F32)
         square = square + part * part
-        total = total + part * gain_ref[t : t + 1, :] * router_ref[t : t + 1, :]
+        total = total + part * router_ref[t : t + 1, :]
     inverse = lax.rsqrt(jnp.sum(square, axis=1, keepdims=True) / (peers * cols) + EPSILON)
     high, low = halves(jnp.sum(total, axis=1, keepdims=True) * inverse)
     row = lax.broadcasted_iota(jnp.int32, (rows, TILE), 0)
@@ -237,6 +246,8 @@
         part = dot(active, down_ref[0, :, t * cols : (t + 2) * cols]).astype(BF16)
         out_ref[t] = part[:, :cols]
         out_ref[t + 1] = part[:, cols:]
+    for copy in copies:
+        copy.wait()
 
 
 def return_kernel(parts_ref, grow_ref, logits_ref, send_ref):
@@ -292,8 +303,8 @@
         decay_rate, frequency, log_step, input_re.transpose(0, 2, 1), input_im.transpose(0, 2, 1)
     )
     expert = lax.axis_index("ep")
-    own_router = lax.dynamic_slice_in_dim(router.T, expert, 1, 0).reshape(peers, cols)
     gain = ffn_gain.reshape(peers, cols)
+    own_router = lax.dynamic_slice_in_dim(router.T, expert, 1, 0).reshape(peers, cols) * gain
     all_resid, place, fetch, pick, keep, grow, own_router, gain = lax.optimization_barrier(
         (all_resid, place, fetch, pick, keep, grow, own_router, gain)
     )
@@ -320,9 +331,15 @@
     arrived = exchange(token_send.reshape(ep_size, per // 2, 2, cols), "ep").reshape(slots, cols)
     tokens_send = call(spread_kernel, shape_of((peers, rows, cols), BF16), arrived, keep)
     tokens = exchange(tokens_send, TP)
-    parts, logits = call(
-        expert_kernel, (shape_of((peers, rows, cols), BF16), shape_of((rows, TILE), BF16)),
-        tokens, gain, own_router, gate_weight, up_weight, down_weight, mib=24,
+    far, near = pl.BlockSpec(memory_space=pl.ANY), pl.BlockSpec(memory_space=pltpu.VMEM)
+    parts, logits, out_re, out_im = call(
+        expert_kernel,
+        (
+            shape_of((peers, rows, cols), BF16), shape_of((rows, TILE), BF16),
+            shape_of(state_re.shape, F32), shape_of(state_im.shape, F32),
+        ),
+        tokens, gain, own_router, gate_weight, up_weight, down_weight, new_re, new_im, mib=24,
+        out_specs=(near, near, far, far), scratch_shapes=[pltpu.SemaphoreType.DMA((2,))],
     )
     own_parts = exchange(parts, TP)
     back_send = call(return_kernel, shape_of((slots, cols), BF16), own_parts, grow, logits)
@@ -330,7 +347,7 @@
     layer_out = call(
         functools.partial(combine_kernel, top), shape_of((seqs, cols), BF16), back, fetch, pick, stream
     )
-    return (layer_out, new_re, new_im)
+    return (layer_out, out_re, out_im)
 
 
 def solution(mesh):

time: 133 us -> 133 us (level)
  no operation moved by 1% of the time
where the time goes in v3:
time: 133 us; the launch traced here: 132 us
  blocking collectives  109 us (82%)
  starting transfers between devices  7.57 us (6%)
  Pallas kernels  5.71 us (4%)
  waiting for transfers between devices  4.13 us (3%)
  local copies, waits for them, and re-layouts  2.45 us (2%)
  other arithmetic  1.83 us (1%)
    all_to_all x6, blocking collectives, exchange(): return lax.all_to_all(blocks, axis, 0, 0, tiled=True)  109 us
    all_to_all x1, starting transfers between devices, exchange(): return lax.all_to_all(blocks, axis, 0, 0, tiled=True)  7.57 us
    pallas_call x8, Pallas kernels, call(): pl.pallas_call(body, out_shape=out, compiler_params=pltpu.CompilerParams(...  5.71 us
    all_to_all x1, waiting for transfers between devices, exchange(): return lax.all_to_all(blocks, axis, 0, 0, tiled=True)  4.13 us
  transfers between devices with their start and end apart: 1, of which 1 were waited for; matrix products, arithmetic and copies ran while one was open for 2% of the time, Pallas kernels for 1%

profile of v3, /device:TPU:1, one launch (start us, length us, event | category | flops | bytes accessed | tf_op | source)
XLA Modules:
  0.0 132.0 jit_solution(14968271443079672146)
XLA Ops:
  0.6 0.0 copy-start
  0.6 0.0 copy-start.10
  0.7 0.0 copy-start.14
  0.7 0.0 copy-start.15
  0.7 0.0 copy-start.12
  0.7 0.0 copy-start.13
  0.7 0.0 copy-start.4
  0.7 0.0 copy-start.11
  0.7 0.0 copy-start.7
  0.7 0.0 copy-start.6
  0.7 1.6 %broadcast_in_dim.8 = bf16[16,64,128]{2,1,0:T(8,128)(2,1)} broadcast(bf16[64,128]{1,0:T(8,128)(2,1)} %resid_ref.1), dimensions={1,2} | broadcast | bytes 278528 | tf_op jit(solution)/shard_map/broadcast_in_dim | solution.py:292
  2.3 7.6 %all-to-all-start = ((bf16[16,64,128]{2,1,0:T(8,128)(2,1)}), bf16[16,64,128]{2,1,0:T(8,128)(2,1)S(1)}, u32[]{:S(2)}, u32[]{:S(2)}) async-start(bf16[16,64,128]{2,1,0:T(8,128)(2,1)} %broadcast_in_dim.8), calls=%async_computation | async-start | bytes 524288 | tf_op jit(solution)/shard_map/all_to_all | solution.py:48
  10.0 0.7 exp.6
  10.6 0.0 copy-done
  10.6 0.8 add_divide_fusion
  11.5 0.8 multiply_add_fusion
  12.3 0.1 maximum_select_fusion.input_re_ref
  12.4 0.0 copy-done.10
  12.4 0.0 copy-done.14
  12.4 0.0 copy-start.8
  12.4 0.0 copy-done.15
  12.4 0.0 copy-done.12
  12.5 0.1 copy.24.route_ref
  12.6 0.8 shard_map.220
  13.3 0.1 maximum_select_fusion.3
  13.4 0.0 copy-start.5
  13.5 0.0 copy-start.9
  13.5 4.1 %all-to-all-done.resid_ref = bf16[16,64,128]{2,1,0:T(8,128)(2,1)S(1)} async-done(((bf16[16,64,128]{2,1,0:T(8,128)(2,1)}), bf16[16,64,128]{2,1,0:T(8,128)(2,1)S(1)}, u32[]{:S(2)}, u32[]{:S(2)}) %all-to-all-start) | async-done | bytes 262176 | tf_op jit(solution)/shard_map/all_to_all | solution.py:48
  17.6 0.0 copy-done.7
  17.6 0.0 copy-done.6
  17.6 1.0 shard_map.221
  18.7 9.6 %all_to_all.35.all_ref = bf16[16,32,128]{2,1,0:T(8,128)(2,1)S(1)} all-to-all(bf16[16,32,128]{2,1,0:T(8,128)(2,1)S(1)} %get-tuple-element.32), channel_id=1, replica_groups=mesh['ep'=32,'tp_0'=4,'tp_1'=4] {'tp_0','tp_1'}, dimensions={0} | all-to-all | bytes 262144 | tf_op jit(solution)/shard_map/all_to_all | solution.py:48
  28.3 0.0 copy-done.8
  28.3 0.3 shard_map.222
  28.6 9.6 %all_to_all.36.all_ref = bf16[16,32,128]{2,1,0:T(8,128)(2,1)S(1)} all-to-all(bf16[16,32,128]{2,1,0:T(8,128)(2,1)S(1)} %shard_map.222), channel_id=1, replica_groups=mesh['ep'=32,'tp_0'=4,'tp_1'=4] {'tp_0','tp_1'}, dimensions={0} | all-to-all | bytes 262144 | tf_op jit(solution)/shard_map/all_to_all | solution.py:48
  38.2 0.0 copy-done.9
  38.2 0.4 shard_map.223
  38.6 33.4 %all_to_all.37 = bf16[32,5,2,128]{3,2,1,0:T(2,128)(2,1)S(1)} all-to-all(bf16[32,5,2,128]{3,2,1,0:T(2,128)(2,1)S(1)} %bitcast.25), channel_id=1, replica_groups=mesh['ep'=32,'tp_0'=4,'tp_1'=4] {'ep'}, dimensions={0} | all-to-all | bytes 163840 | tf_op jit(solution)/shard_map/all_to_all | solution.py:48
  72.0 0.3 shard_map.224
  72.3 0.0 copy-start.1
  72.3 0.0 copy-start.2
  72.3 24.4 %all_to_all.38.tokens_ref = bf16[16,288,128]{2,1,0:T(8,128)(2,1)S(1)} all-to-all(bf16[16,288,128]{2,1,0:T(8,128)(2,1)S(1)} %shard_map.224), channel_id=1, replica_groups=mesh['ep'=32,'tp_0'=4,'tp_1'=4] {'tp_0','tp_1'}, dimensions={0} | all-to-all | bytes 2359296 | tf_op jit(solution)/shard_map/all_to_all | solution.py:48
  96.7 0.0 copy-done.2
  96.7 1.6 %shard_map.225 = (bf16[16,288,128]{2,1,0:T(8,128)(2,1)S(1)}, bf16[288,128]{1,0:T(8,128)(2,1)S(1)}, f32[64,4,64]{2,1,0:T(4,128)}, f32[64,4,64]{2,1,0:T(4,128)}) custom-call(bf16[16,288,128]{2,1,0:T(8,128)(2,1)S(1)} %all_to_all.38.tokens_ref, f32[16,128]{1,0:T(8,128)S(1)} %bitcast.26, f32[16,128]{1,0:T(8,128)S(1)} %bitcast_multiply_fusion.router_ref, ...), custom_call_target="tpu_custom_call" | custom-call | tf_op jit(solution)/shard_map/pallas_call | solution.py:22
  98.3 16.7 %all_to_all.39.parts_ref = bf16[16,288,128]{2,1,0:T(8,128)(2,1)S(1)} all-to-all(bf16[16,288,128]{2,1,0:T(8,128)(2,1)S(1)} %get-tuple-element.41), channel_id=1, replica_groups=mesh['ep'=32,'tp_0'=4,'tp_1'=4] {'tp_0','tp_1'}, dimensions={0} | all-to-all | bytes 2359296 | tf_op jit(solution)/shard_map/all_to_all | solution.py:48
  115.0 0.4 shard_map.226
  115.4 15.7 %all_to_all.40 = bf16[32,5,2,128]{3,2,1,0:T(2,128)(2,1)S(1)} all-to-all(bf16[32,5,2,128]{3,2,1,0:T(2,128)(2,1)S(1)} %bitcast.20), channel_id=1, replica_groups=mesh['ep'=32,'tp_0'=4,'tp_1'=4] {'ep'}, dimensions={0} | all-to-all | bytes 163840 | tf_op jit(solution)/shard_map/all_to_all | solution.py:48
  131.1 1.0 shard_map.227
  (17 shorter events, 0.1 us)
Async XLA Ops:
  0.6 10.0 %copy-start = (f32[2048,32]{0,1:T(8,128)S(1)}, f32[2048,32]{0,1:T(8,128)}, u32[]{:S(2)}) copy-start(f32[2048,32]{0,1:T(8,128)} %param.37) | copy-start | bytes 786436
  0.6 11.7 %copy-start.10 = (f32[2048]{0:T(1024)S(1)}, f32[2048]{0:T(1024)}, u32[]{:S(2)}) copy-start(f32[2048]{0:T(1024)} %param.36) | copy-start | bytes 24580
  0.7 11.7 %copy-start.14 = (f32[4,16,64]{2,1,0:T(8,128)S(1)}, f32[4,16,64]{2,1,0:T(8,128)}, u32[]{:S(2)}) copy-start(f32[4,16,64]{2,1,0:T(8,128)} %param.31) | copy-start | bytes 49156
  0.7 11.8 %copy-start.15 = (f32[4,16,64]{2,1,0:T(8,128)S(1)}, f32[4,16,64]{2,1,0:T(8,128)}, u32[]{:S(2)}) copy-start(f32[4,16,64]{2,1,0:T(8,128)} %param.32) | copy-start | bytes 49156
  0.7 11.8 %copy-start.12 = (s32[64,4]{0,1:T(4,128)S(1)}, s32[64,4]{0,1:T(4,128)}, u32[]{:S(2)}) copy-start(s32[64,4]{0,1:T(4,128)} %param.41) | copy-start | bytes 3076
  0.7 16.9 %copy-start.13 = (f32[64]{0:T(128)S(1)}, f32[64]{0:T(128)}, u32[]{:S(2)}) copy-start(f32[64]{0:T(128)} %param.33) | copy-start | bytes 772
  0.7 16.9 %copy-start.4 = (bf16[2048,64]{0,1:T(8,128)(2,1)S(1)}, bf16[2048,64]{0,1:T(8,128)(2,1)}, u32[]{:S(2)}) copy-start(bf16[2048,64]{0,1:T(8,128)(2,1)} %param.25) | copy-start | bytes 786436
  0.7 16.9 %copy-start.11 = (f32[2048]{0:T(1024)S(1)}, f32[2048]{0:T(1024)}, u32[]{:S(2)}) copy-start(f32[2048]{0:T(1024)} %param.24) | copy-start | bytes 24580
  0.7 16.9 %copy-start.7 = (f32[64,4,64]{2,1,0:T(4,128)S(1)}, f32[64,4,64]{2,1,0:T(4,128)}, u32[]{:S(2)}) copy-start(f32[64,4,64]{2,1,0:T(4,128)} %state_im_ref.1) | copy-start | bytes 196612
  0.7 16.9 %copy-start.6 = (f32[64,4,64]{2,1,0:T(4,128)S(1)}, f32[64,4,64]{2,1,0:T(4,128)}, u32[]{:S(2)}) copy-start(f32[64,4,64]{2,1,0:T(4,128)} %state_re_ref.1) | copy-start | bytes 196612
  2.3 15.3 %all-to-all-start = ((bf16[16,64,128]{2,1,0:T(8,128)(2,1)}), bf16[16,64,128]{2,1,0:T(8,128)(2,1)S(1)}, u32[]{:S(2)}, u32[]{:S(2)}) async-start(bf16[16,64,128]{2,1,0:T(8,128)(2,1)} %broadcast_in_dim.8), calls=%async_computation | async-start | bytes 524288 | tf_op jit(solution)/shard_map/all_to_all | solution.py:48
  12.4 15.9 %copy-start.8 = (bf16[1024,64]{0,1:T(8,128)(2,1)S(1)}, bf16[1024,64]{0,1:T(8,128)(2,1)}, u32[]{:S(2)}) copy-start(bf16[1024,64]{0,1:T(8,128)(2,1)} %param.34) | copy-start | bytes 393220
  13.4 24.8 %copy-start.5 = (bf16[1024,128]{1,0:T(8,128)(2,1)S(1)}, bf16[1024,128]{1,0:T(8,128)(2,1)}, u32[]{:S(2)}) copy-start(bf16[1024,128]{1,0:T(8,128)(2,1)} %weight_ref.1) | copy-start | bytes 786436
  13.5 24.8 %copy-start.9 = (bf16[64,128]{1,0:T(8,128)(2,1)S(1)}, bf16[64,128]{1,0:T(8,128)(2,1)}, u32[]{:S(2)}) copy-start(bf16[64,128]{1,0:T(8,128)(2,1)} %resid_ref.1) | copy-start | bytes 49156
  72.0 24.7 %copy-start.3 = (bf16[1,256,2048]{2,1,0:T(8,128)(2,1)S(1)}, bf16[1,256,2048]{2,1,0:T(8,128)(2,1)}, u32[]{:S(2)}) copy-start(bf16[1,256,2048]{2,1,0:T(8,128)(2,1)} %down_ref.1) | copy-start | bytes 3145732
  72.3 24.4 %copy-start.1 = (bf16[1,2048,256]{2,1,0:T(8,128)(2,1)S(1)}, bf16[1,2048,256]{2,1,0:T(8,128)(2,1)}, u32[]{:S(2)}) copy-start(bf16[1,2048,256]{2,1,0:T(8,128)(2,1)} %gate_ref.1) | copy-start | bytes 3145732
  72.3 24.4 %copy-start.2 = (bf16[1,2048,256]{2,1,0:T(8,128)(2,1)S(1)}, bf16[1,2048,256]{2,1,0:T(8,128)(2,1)}, u32[]{:S(2)}) copy-start(bf16[1,2048,256]{2,1,0:T(8,128)(2,1)} %up_ref.1) | copy-start | bytes 3145732
